TPU v7x, 32 devices: a whole 2x2x4 slice. The times are simulated.
32 devices in a mesh: sp: 16 (over z, y, x), tp: 2 (over core).
Axes of the slice: x: 2, y: 2, z: 4, core: 2. Of those that a mesh axis runs over, the one named last changes fastest.
Arguments:
- layer_source_tokens: bfloat16 [2, 1024, 4096], P(None, 'sp'), may hold values from -6 to 6
- address_projection: bfloat16 [4096, 2048], P('sp', 'tp'), may hold values from -0.09375 to 0.09375
- content_projection: bfloat16 [4096, 2048], P('sp', 'tp'), may hold values from -0.09375 to 0.09375
- strength_projection: bfloat16 [4096, 16], replicated, may hold values from -0.09375 to 0.09375
- fading_driver_projection: bfloat16 [4096, 16], replicated, may hold values from -0.25 to 0.25
- strength_offset: float32 [16], P('tp'), may hold values from -2.5 to 1
- channel_fading_speed: float32 [16], P('tp')
- added_fading_exponent: float32 [2, 1024, 16], P(None, 'sp', 'tp'), may hold values from -0.7 to 0, as said below
- first_step_probe: bfloat16 [2, 2048], P(None, 'tp'), may hold values from -6 to 6
- first_step_address: bfloat16 [2, 2048], P(None, 'tp'), may hold values from -6 to 6
- first_step_content: bfloat16 [2, 2048], P(None, 'tp'), may hold values from -6 to 6
- first_step_outgate: bfloat16 [2, 2048], P(None, 'tp'), may hold values from -6 to 6
- first_step_strength_raw: float32 [2, 16], P(None, 'tp'), may hold values from -6 to 6
- channel_scaling_factor: float32 [128], replicated, may hold values from 0.1 to 1.9
- readout_projection: bfloat16 [2048, 4096], P('tp', 'sp'), may hold values from -0.125 to 0.125
Outputs:
- state_cache: bfloat16 [2, 16, 128, 128], P(None, 'tp')
- mixed_read: bfloat16 [2, 4096], P(None, 'sp')
- boundary_cache: bfloat16 [2, 16, 16, 128, 128], P(None, 'sp', 'tp')
Inputs may be any that keep to these rules, and one draw needn't show every extreme that they name: `added_fading_exponent`: zero at most positions.
All inputs are finite; a program needn't handle non-finite values.
Results may differ from a plain program's by a relative error of at most 0.017.
Values may be sent and summed in bfloat16 or wider, within the bound.
A program may use at most 64 MiB of HBM per device.

v0:
```python
import jax
import jax.numpy as jnp
from jax import lax
from jax.experimental import pallas as pl
from jax.experimental.pallas import tpu as pltpu
from jax.sharding import PartitionSpec as P

ADDRESS_WIDTH = 128
BLOCK = 64


EPSILON = 1e-06
HIGHEST_ACCURACY = lax.Precision.HIGHEST


def prefix(array, axis, combine, identity):
    peers, index = (lax.axis_size(axis), lax.axis_index(axis))
    everything = jax.tree.map(
        lambda part, kind: lax.all_gather(part.astype(kind), axis),
        array,
        (jnp.bfloat16, jnp.bfloat16),
    )
    start = jax.tree.map(
        lambda part, zero: jnp.broadcast_to(jnp.asarray(zero, part.dtype), part.shape),
        array,
        identity,
    )

    def step(k, before):
        reached = k < index
        new = combine(
            before, jax.tree.map(lambda part, own: part[k].astype(own.dtype), everything, array)
        )
        return jax.tree.map(lambda a, b: jnp.where(reached, a, b), new, before)

    return lax.fori_loop(0, peers, step, start)


def as_sent(array):
    return jax.tree.map(lambda a: a.astype(jnp.bfloat16) if a.dtype == jnp.float32 else a, array)


def broadcast(value, axis, source):
    kept = jnp.where(lax.axis_index(axis) == source, value, 0).astype(value.dtype)
    return lax.psum(kept, axis)


def unit_inverse(lower_part):
    matrix_order = lower_part.shape[-1]
    identity = jnp.eye(matrix_order, dtype=jnp.float32)
    result = identity - lower_part
    power_term = lower_part
    reached = 2
    while reached < matrix_order:
        power_term = jnp.matmul(power_term, power_term, precision=HIGHEST_ACCURACY)
        result = jnp.matmul(result, identity + power_term, precision=HIGHEST_ACCURACY)
        reached = reached * 2
    return result


def build_arguments(
    address_vectors,
    content_vectors,
    outgate_raw_scores,
    strength_offset,
    channel_fading_speed,
    added_fading_exponent,
    channel_width,
):
    length = address_vectors.shape[0]
    attention_channels_total = channel_fading_speed.shape[0]
    address_token_slab = jax.nn.silu(address_vectors.astype(jnp.float32)).reshape(
        length, attention_channels_total, channel_width
    )
    address_token_slab = address_token_slab * lax.rsqrt(
        jnp.sum(address_token_slab * address_token_slab, axis=-1, keepdims=True) + EPSILON
    )
    content_token_slab = jax.nn.silu(content_vectors.astype(jnp.float32)).reshape(
        length, attention_channels_total, channel_width
    )
    strength_raw_expanded = outgate_raw_scores.astype(jnp.float32)
    storing_strength = jax.nn.sigmoid(
        strength_raw_expanded[:, :attention_channels_total] + strength_offset
    )
    fading_exponent = added_fading_exponent - channel_fading_speed * jax.nn.softplus(
        strength_raw_expanded[:, attention_channels_total:]
    )
    return (address_token_slab, content_token_slab, storing_strength, fading_exponent)


def range_map(address_token_slab, content_token_slab, storing_strength, fading_exponent, block):
    length, attention_channels_total, channel_width = address_token_slab.shape
    blocks = length // block

    def split_blocks(tensor):
        moved_axes = jnp.swapaxes(tensor, 0, 1)
        return moved_axes.reshape((attention_channels_total, blocks, block) + moved_axes.shape[2:])

    block_keys = split_blocks(address_token_slab)
    block_values = split_blocks(content_token_slab)
    block_beta = split_blocks(storing_strength)
    cumulative = jnp.cumsum(split_blocks(fading_exponent), axis=-1)
    positions = jnp.arange(block)
    strict = positions[:, None] > positions[None, :]
    spread_log = jnp.where(strict, cumulative[..., :, None] - cumulative[..., None, :], 0.0)
    scaled_keys = block_keys * block_beta[..., None]
    inner_prod = jnp.einsum("hnik,hnjk->hnij", scaled_keys, block_keys, precision=HIGHEST_ACCURACY)
    lower_part = jnp.where(strict, inner_prod * jnp.exp(spread_log), 0.0)
    inverse = unit_inverse(lower_part)
    targets = jnp.concatenate(
        [block_values * block_beta[..., None], scaled_keys * jnp.exp(cumulative)[..., None]],
        axis=-1,
    )
    solved = jnp.einsum("hnij,hnjk->hnik", inverse, targets, precision=HIGHEST_ACCURACY)
    updates = solved[..., :channel_width]
    key_weights = solved[..., channel_width:]
    tail_keys = block_keys * jnp.exp(cumulative[..., -1:] - cumulative)[..., None]
    last_decay = jnp.exp(cumulative[..., -1])
    identity = jnp.eye(channel_width, dtype=jnp.float32)

    def advance(state_pair, block_items):
        transition, carried_state = state_pair
        update_index, weight_index, tail_index, last_index = block_items
        fresh_value_rows = update_index - jnp.einsum(
            "xbg,xgp->xbp", weight_index, carried_state, precision=HIGHEST_ACCURACY
        )
        carried_state = carried_state * last_index[:, None, None] + jnp.einsum(
            "tjo,tjw->tow", tail_index, fresh_value_rows, precision=HIGHEST_ACCURACY
        )
        block_move = last_index[:, None, None] * identity - jnp.einsum(
            "hck,hcj->hkj", tail_index, weight_index, precision=HIGHEST_ACCURACY
        )
        transition = jnp.einsum("hij,hjk->hik", block_move, transition, precision=HIGHEST_ACCURACY)
        return ((transition, carried_state), None)

    initial = (
        jnp.broadcast_to(identity, (attention_channels_total, channel_width, channel_width)),
        jnp.zeros((attention_channels_total, channel_width, channel_width), jnp.float32),
    )
    block_items = (
        jnp.moveaxis(updates, 1, 0),
        jnp.moveaxis(key_weights, 1, 0),
        jnp.moveaxis(tail_keys, 1, 0),
        jnp.moveaxis(last_decay, 1, 0),
    )
    (transition, carried_state), _ = lax.scan(advance, initial, block_items)
    return (transition, carried_state)


def read_heads(
    state_cache,
    first_step_probe,
    first_step_address,
    first_step_content,
    first_step_outgate,
    first_step_strength_raw,
    channel_scaling_factor,
):
    seq_count, attention_channels_total, channel_width, _ = state_cache.shape
    carried_state = state_cache.astype(jnp.float32)

    def activate(tensor):
        return jax.nn.silu(tensor.astype(jnp.float32)).reshape(
            seq_count, attention_channels_total, channel_width
        )

    query_rows = activate(first_step_probe)
    address_token_slab = activate(first_step_address)
    address_token_slab = address_token_slab * lax.rsqrt(
        jnp.sum(address_token_slab * address_token_slab, axis=-1, keepdims=True) + EPSILON
    )
    content_token_slab = activate(first_step_content)
    storing_strength = jax.nn.sigmoid(first_step_strength_raw)
    recalled = jnp.einsum(
        "nhk,nhkv->nhv", address_token_slab, carried_state, precision=HIGHEST_ACCURACY
    )
    updated = (
        carried_state
        + storing_strength[..., None, None]
        * address_token_slab[..., :, None]
        * (content_token_slab - recalled)[..., None, :]
    )
    output = jnp.einsum("nhk,nhkv->nhv", query_rows, updated, precision=HIGHEST_ACCURACY)
    normed = (
        output
        * lax.rsqrt(jnp.mean(output * output, axis=-1, keepdims=True) + EPSILON)
        * channel_scaling_factor
    )
    gated_out = normed * activate(first_step_outgate)
    return gated_out.reshape(seq_count, attention_channels_total * channel_width).astype(
        jnp.bfloat16
    )


def matmul_maps(left, right):
    return jnp.einsum("shij,shjk->shik", left, right, precision=HIGHEST_ACCURACY)


def join_pairs(earlier, later):
    return (matmul_maps(later[0], earlier[0]), matmul_maps(later[0], earlier[1]) + later[1])


def per_device(
    layer_source_tokens,
    address_projection,
    content_projection,
    strength_projection,
    fading_driver_projection,
    strength_offset,
    channel_fading_speed,
    added_fading_exponent,
    first_step_probe,
    first_step_address,
    first_step_content,
    first_step_outgate,
    first_step_strength_raw,
    channel_scaling_factor,
    readout_projection,
):
    head_local = channel_fading_speed.shape[0]
    first_head = lax.axis_index("tp") * head_local
    beta_slice = lax.dynamic_slice_in_dim(strength_projection, first_head, head_local, 1)
    alpha_slice = lax.dynamic_slice_in_dim(fading_driver_projection, first_head, head_local, 1)
    seq_count, local_len, model_width = layer_source_tokens.shape
    flat_rows = layer_source_tokens.reshape(seq_count * local_len, model_width)
    key_sum = jnp.dot(
        flat_rows,
        lax.all_gather(address_projection, "sp", axis=0, tiled=True),
        preferred_element_type=jnp.float32,
    )
    value_sum = jnp.dot(
        flat_rows,
        lax.all_gather(content_projection, "sp", axis=0, tiled=True),
        preferred_element_type=jnp.float32,
    )
    beta_sum = jnp.dot(flat_rows, beta_slice, preferred_element_type=jnp.float32)
    alpha_sum = jnp.dot(flat_rows, alpha_slice, preferred_element_type=jnp.float32)
    outgate_raw_scores = (
        jnp.concatenate([beta_sum, alpha_sum], axis=1)
        .astype(jnp.bfloat16)
        .reshape(seq_count, local_len, -1)
    )
    address_vectors = key_sum.astype(jnp.bfloat16).reshape(seq_count, local_len, -1)
    content_vectors = value_sum.astype(jnp.bfloat16).reshape(seq_count, local_len, -1)
    transitions = []
    offsets = []
    for prompt_number in range(seq_count):
        address_token_slab, content_token_slab, storing_strength, fading_exponent = build_arguments(
            address_vectors[prompt_number],
            content_vectors[prompt_number],
            outgate_raw_scores[prompt_number],
            strength_offset,
            channel_fading_speed,
            added_fading_exponent[prompt_number],
            ADDRESS_WIDTH,
        )
        transition, carried_state = range_map(
            address_token_slab, content_token_slab, storing_strength, fading_exponent, BLOCK
        )
        transitions.append(transition)
        offsets.append(carried_state)
    transition = jnp.stack(transitions)
    offset = jnp.stack(offsets)
    identity = jnp.broadcast_to(jnp.eye(ADDRESS_WIDTH, dtype=jnp.float32), transition.shape)
    entered = prefix((transition, offset), "sp", join_pairs, (identity, jnp.zeros_like(offset)))
    leaving = matmul_maps(transition, entered[1]) + offset
    final = broadcast(as_sent(leaving), "sp", lax.axis_size("sp") - 1).astype(leaving.dtype)
    boundary_cache = leaving.astype(jnp.bfloat16)[:, None]
    state_cache = final.astype(jnp.bfloat16)
    heads_read = read_heads(
        state_cache,
        first_step_probe,
        first_step_address,
        first_step_content,
        first_step_outgate,
        first_step_strength_raw,
        channel_scaling_factor,
    )
    group_terms = jnp.dot(
        heads_read, readout_projection, preferred_element_type=jnp.float32
    ).astype(jnp.bfloat16)
    mixed_read = lax.psum(group_terms.astype(jnp.float32).astype(jnp.bfloat16), "tp")
    return (state_cache, mixed_read, boundary_cache)


MESH = pl.DeviceIdType.MESH
PIECES = 2


def remote(src, dst, send, recv, sp, tp):
    return pltpu.make_async_remote_copy(
        src_ref=src,
        dst_ref=dst,
        send_sem=send,
        recv_sem=recv,
        device_id={"sp": sp, "tp": tp},
        device_id_type=MESH,
    )


def gather_kernel(
    peers,
    tok,
    wk,
    wv,
    add,
    gates,
    out,
    addall,
    xall,
    wall,
    keep,
    give,
    got,
    own_sem,
    across_send,
    a_send,
    b_send,
    tok_recv,
    w_send,
    w_recv,
    relay_send,
    relay_recv,
    add_send,
    add_recv,
    give_send,
    give_recv,
):
    s, t = lax.axis_index("sp"), lax.axis_index("tp")
    ring = peers // 2
    x, q = s % 2, s // 2
    half = tok.shape[2] // 2
    length = tok.shape[1]
    piece = length // PIECES
    rows = wk.shape[0]
    width = ADDRESS_WIDTH
    columns = pl.ds(pl.multiple_of(t * half, 128), half)

    def place(r):
        y = r // (ring // 2)
        z = (1 - y) * r + y * (ring - 1 - r)
        return 2 * z + y

    y, z = q % 2, q // 2
    r = (1 - y) * z + y * (ring - 1 - z)
    after = place((r + 1) % ring)
    before = place((r + ring - 1) % ring)

    def part(i):
        return pl.ds(i * piece, piece)

    def token_wait(slot, i):
        ref = xall.at[slot, part(i)]
        remote(ref, ref, across_send.at[i], tok_recv.at[slot, i], s, t).wait_recv()

    sent = []

    def go(copy):
        copy.start()
        sent.append(copy)

    for i in range(PIECES):
        go(
            remote(
                tok.at[1 - x, part(i), columns],
                xall.at[s, part(i)],
                across_send.at[i],
                tok_recv.at[s, i],
                2 * q + 1 - x,
                t,
            )
        )
        go(
            remote(
                tok.at[x, part(i), columns],
                xall.at[s, part(i)],
                a_send.at[0, i],
                tok_recv.at[s, i],
                2 * after + x,
                t,
            )
        )
    own = pltpu.make_async_copy(tok.at[x, :, columns], xall.at[s], own_sem)
    own.start()

    side = s // ring
    other = (t + side) % 2
    row_slot = s % ring
    spot = pl.ds(pl.multiple_of(row_slot * rows, 16), rows)
    for off in range(ring):
        head = (q + off) % ring
        for kv, w in enumerate((wk, wv)):
            src = w.at[:, pl.ds(pl.multiple_of(head * width, 128), width)]
            dst = wall.at[spot, pl.ds(pl.multiple_of((2 * other + kv) * width, 128), width)]
            copy = remote(
                src, dst, w_send.at[off, kv], w_recv.at[row_slot, 2 * other + kv], 2 * head + x, side
            )
            if off == 0:

                @pl.when(t == side)
                def _():
                    pltpu.make_async_copy(src, dst, w_recv.at[row_slot, 2 * other + kv]).start()

                @pl.when(t != side)
                def _():
                    copy.start()
            else:
                go(copy)

    for off in range(1, peers):
        to = (s + off) % peers
        go(remote(add.at[to % 2], addall.at[s], add_send.at[off], add_recv.at[s], to, t))
    own_add = pltpu.make_async_copy(add.at[x], addall.at[s], add_recv.at[s])
    own_add.start()

    def relay(m):
        slot = 2 * m + x
        block = wall.at[pl.ds(pl.multiple_of(slot * rows, 16), rows)]
        for c in range(4):
            one = wall.at[pl.ds(pl.multiple_of(slot * rows, 16), rows), pl.ds(c * width, width)]
            pltpu.make_async_copy(one, one, w_recv.at[slot, c]).wait()
        go(remote(block, block, relay_send.at[m], relay_recv.at[slot], 2 * q + 1 - x, t))

    relays = list(range(ring // 2))
    for k in range(ring - 1):
        for i in range(PIECES):
            if k > 0:
                slot = 2 * place((r - k + ring) % ring) + x
                token_wait(slot, i)
                ref = xall.at[slot, part(i)]
                go(remote(ref, ref, a_send.at[k, i], tok_recv.at[slot, i], 2 * after + x, t))
            slot = 2 * place((r + k) % ring) + 1 - x
            token_wait(slot, i)
            ref = xall.at[slot, part(i)]
            go(remote(ref, ref, b_send.at[k, i], tok_recv.at[slot, i], 2 * before + x, t))
        if k >= 2 and relays:
            relay(relays.pop(0))
    while relays:
        relay(relays.pop(0))
    for m in range(ring // 2):
        slot = 2 * m + 1 - x
        block = wall.at[pl.ds(pl.multiple_of(slot * rows, 16), rows)]
        remote(block, block, relay_send.at[m], relay_recv.at[slot], s, t).wait_recv()
    own.wait()

    def project(g):
        slots = []
        for k in (2 * g, 2 * g + 1):
            slots.append(2 * place((r - k + ring) % ring) + x)
            slots.append(2 * place((r + k) % ring) + 1 - x)
        rows_in = jnp.concatenate([xall[slot] for slot in slots], axis=0)
        wide = jnp.dot(rows_in, wall[...], preferred_element_type=jnp.float32)
        logits = jnp.dot(rows_in, gates[...], preferred_element_type=jnp.float32)
        for i, slot in enumerate(slots):
            part_of = slice(i * length, (i + 1) * length)
            keep[slot, :, : 2 * width] = wide[part_of, : 2 * width]
            keep[slot, :, 2 * width :] = logits[part_of]
            give[slot, :, : 2 * width] = wide[part_of, 2 * width :]
            give[slot, :, 2 * width :] = logits[part_of]
        for slot in slots:
            remote(
                give.at[slot], got.at[slot], give_send.at[slot], give_recv.at[slot], s, 1 - t
            ).start()

    lax.fori_loop(0, ring // 2 - 1, lambda g, c: (project(g), c)[1], 0)
    for i in range(PIECES):
        token_wait(2 * place((r + 1) % ring) + x, i)
        token_wait(2 * place((r + ring - 1) % ring) + 1 - x, i)
    project(ring // 2 - 1)
    for off in range(peers):
        slot = (s + off) % peers
        pltpu.make_async_copy(addall.at[slot], addall.at[slot], add_recv.at[slot]).wait()
    for copy in sent:
        copy.wait_send()

    def finish(slot, c):
        copy = remote(
            give.at[slot], got.at[slot], give_send.at[slot], give_recv.at[slot], s, 1 - t
        )
        copy.wait_recv()
        out[slot] = (keep[slot] + got[slot]).astype(out.dtype)
        copy.wait_send()
        return c

    lax.fori_loop(0, peers, finish, 0)

    @pl.when(t != side)
    def _():
        for kv, w in enumerate((wk, wv)):
            src = w.at[:, pl.ds(pl.multiple_of(q * width, 128), width)]
            dst = wall.at[spot, pl.ds(pl.multiple_of((2 * other + kv) * width, 128), width)]
            remote(
                src, dst, w_send.at[0, kv], w_recv.at[row_slot, 2 * other + kv], 2 * q + x, side
            ).wait_send()


def gather_inputs(tok, wk, wv, add, gates, peers):
    seq_count, length, model_width = tok.shape
    ring = peers // 2
    heads = add.shape[1]
    dma = pltpu.SemaphoreType.DMA
    anywhere = pl.BlockSpec(memory_space=pl.ANY)
    vmem = pl.BlockSpec(memory_space=pltpu.VMEM)
    return pl.pallas_call(
        lambda *refs: gather_kernel(peers, *refs),
        out_shape=(
            jax.ShapeDtypeStruct((peers, length, 2 * ADDRESS_WIDTH + gates.shape[1]), tok.dtype),
            jax.ShapeDtypeStruct((peers, heads, length), add.dtype),
        ),
        in_specs=[anywhere] * 4 + [vmem],
        out_specs=(vmem, vmem),
        scratch_shapes=[
            pltpu.VMEM((peers, length, model_width // 2), tok.dtype),
            pltpu.VMEM((model_width // 2, 4 * ADDRESS_WIDTH), wk.dtype),
            pltpu.VMEM((peers, length, 2 * ADDRESS_WIDTH + gates.shape[1]), jnp.float32),
            pltpu.VMEM((peers, length, 2 * ADDRESS_WIDTH + gates.shape[1]), jnp.float32),
            pltpu.VMEM((peers, length, 2 * ADDRESS_WIDTH + gates.shape[1]), jnp.float32),
            dma(()),
            dma((PIECES,)),
            dma((ring - 1, PIECES)),
            dma((ring - 1, PIECES)),
            dma((peers, PIECES)),
            dma((ring, 2)),
            dma((ring, 4)),
            dma((ring // 2,)),
            dma((ring,)),
            dma((peers,)),
            dma((peers,)),
            dma((peers,)),
            dma((peers,)),
        ],
        compiler_params=pltpu.CompilerParams(has_side_effects=True),
        name="gather_inputs",
    )(tok, wk, wv, add, gates)


def spread_kernel(peers, states, final, bound, f_send, f_recv, b_send, b_recv):
    s, t = lax.axis_index("sp"), lax.axis_index("tp")
    ring = peers // 2
    slot = (s % 2) * ring + s // 2
    x, q = s % 2, s // 2
    y, z = q % 2, q // 2
    deep = ring // 2
    sent = []

    def go(copy):
        copy.start()
        sent.append(copy)

    def pass_on(slot_of, src, to, sem):
        go(remote(src, final.at[slot_of], f_send.at[sem], f_recv.at[slot_of], to, t))

    def arrived(slot_of):
        ref = final.at[slot_of]
        remote(ref, ref, f_send.at[0], f_recv.at[slot_of], s, t).wait_recv()

    own = states.at[peers - 1]
    y_peer, x_peer = 4 * z + 2 * (1 - y) + x, 2 * q + 1 - x
    for off in range(1, deep):
        pass_on(slot, own, 4 * ((z + off) % deep) + 2 * y + x, off)
    pass_on(slot, own, y_peer, deep)
    pass_on(slot, own, x_peer, 2 * deep)
    final[slot] = states[peers - 1]
    for off in range(1, peers):
        to = (s + off) % peers
        go(remote(states.at[to], bound.at[slot], b_send.at[off], b_recv.at[slot], to, t))
    bound[slot] = states[s]
    for off in range(1, deep):
        come = x * ring + 2 * ((z + off) % deep) + y
        arrived(come)
        pass_on(come, final.at[come], y_peer, deep + off)
        pass_on(come, final.at[come], x_peer, 2 * deep + off)
    for off in range(deep):
        come = x * ring + 2 * ((z + off) % deep) + 1 - y
        arrived(come)
        pass_on(come, final.at[come], x_peer, 3 * deep + off)
    for off in range(ring):
        arrived((1 - x) * ring + (q + off) % ring)
    for off in range(1, peers):
        other = (s + off) % peers
        ref = bound.at[(other % 2) * ring + other // 2]
        remote(
            ref, ref, b_send.at[off], b_recv.at[(other % 2) * ring + other // 2], s, t
        ).wait_recv()
    for copy in sent:
        copy.wait_send()


def spread_states(states, peers):
    dma = pltpu.SemaphoreType.DMA
    vmem = pl.BlockSpec(memory_space=pltpu.VMEM)
    return pl.pallas_call(
        lambda *refs: spread_kernel(peers, *refs),
        out_shape=(jax.ShapeDtypeStruct(states.shape, states.dtype),) * 2,
        in_specs=[vmem],
        out_specs=(vmem, vmem),
        scratch_shapes=[dma((peers,))] * 4,
        compiler_params=pltpu.CompilerParams(has_side_effects=True),
        name="spread_states",
    )(states)


def dot32(spec, a, b):
    return jnp.einsum(spec, a, b, precision=lax.Precision.HIGH)


def block_inverse(lower):
    order = lower.shape[-1]
    identity = jnp.eye(order, dtype=jnp.float32)
    result, power = identity - lower, lower
    reached = 2
    while reached < order:
        power = dot32("nij,njk->nik", power, power)
        result = dot32("nij,njk->nik", result, identity + power)
        reached = reached * 2
    return result


def block_states(keys, values, beta, fading):
    blocks, block, width = keys.shape
    cumulative = jnp.cumsum(fading, axis=-1)
    positions = jnp.arange(block)
    strict = positions[:, None] > positions[None, :]
    spread_log = jnp.where(strict, cumulative[:, :, None] - cumulative[:, None, :], 0.0)
    scaled_keys = keys * beta[..., None]
    inner = dot32("nik,njk->nij", scaled_keys, keys)
    inverse = block_inverse(jnp.where(strict, inner * jnp.exp(spread_log), 0.0))
    targets = jnp.concatenate(
        [scaled_keys * jnp.exp(cumulative)[..., None], values * beta[..., None]], axis=-1
    )
    solved = dot32("nij,njk->nik", inverse, targets)
    tail = keys * jnp.exp(cumulative[:, -1:] - cumulative)[..., None]
    maps = dot32("nck,ncj->nkj", tail, solved)
    last = jnp.exp(cumulative[:, -1])[:, None, None]
    moves = last * jnp.eye(width, dtype=jnp.float32) - maps[..., :width]
    pair = jnp.concatenate([moves, maps[..., width:]], axis=-1)
    zero = jnp.zeros((blocks, width, width), jnp.float32)
    reach = 1
    while reach < blocks:
        late = pair[reach:]
        joined = dot32("nij,njk->nik", late[..., :width], pair[:-reach])
        joined = joined + jnp.concatenate([zero[reach:], late[..., width:]], axis=-1)
        pair = jnp.concatenate([pair[:reach], joined], axis=0)
        reach *= 2
    return pair[..., width:]


def per_device_heads(
    layer_source_tokens,
    address_projection,
    content_projection,
    strength_projection,
    fading_driver_projection,
    strength_offset,
    channel_fading_speed,
    added_fading_exponent,
    first_step_probe,
    first_step_address,
    first_step_content,
    first_step_outgate,
    first_step_strength_raw,
    channel_scaling_factor,
    readout_projection,
):
    peers = lax.axis_size("sp")
    head_local = channel_fading_speed.shape[0]
    s, t = lax.axis_index("sp"), lax.axis_index("tp")
    mine = s // 2
    _, length, model_width = layer_source_tokens.shape
    half = model_width // 2
    width = ADDRESS_WIDTH
    gates = jnp.concatenate([strength_projection, fading_driver_projection], axis=1)
    gates = lax.dynamic_slice_in_dim(gates, t * half, half, 0)
    gate_count = gates.shape[1]
    gates = jnp.pad(gates, ((0, 0), (0, -gate_count % 128)))
    projected, added = gather_inputs(
        layer_source_tokens,
        address_projection,
        content_projection,
        jnp.swapaxes(added_fading_exponent, 1, 2),
        gates,
        peers,
    )
    projected = projected.astype(jnp.float32)
    wide = projected[..., : 2 * width]
    gate_sum = projected[..., 2 * width :].reshape(peers * length, -1)
    acted = jax.nn.silu(wide)
    keys = acted[..., :width]
    keys = keys * lax.rsqrt(jnp.sum(keys * keys, axis=-1, keepdims=True) + EPSILON)
    values = acted[..., width:]
    head = t * head_local + mine
    total_heads = strength_projection.shape[1]
    beta_logit = lax.dynamic_slice_in_dim(gate_sum, head, 1, 1).reshape(peers, length)
    alpha_logit = lax.dynamic_slice_in_dim(gate_sum, total_heads + head, 1, 1).reshape(
        peers, length
    )
    beta = jax.nn.sigmoid(beta_logit + lax.dynamic_index_in_dim(strength_offset, mine, 0))
    added_own = lax.dynamic_index_in_dim(added, mine, 1, keepdims=False)
    speed = lax.dynamic_index_in_dim(channel_fading_speed, mine, 0)
    fading = added_own - speed * jax.nn.softplus(alpha_logit)
    states = block_states(keys, values, beta, fading).astype(jnp.bfloat16)
    final, bound = spread_states(states, peers)
    state_cache = final.reshape(2, head_local, width, width)
    boundary_cache = bound.reshape(2, 1, head_local, width, width)
    heads_read = read_heads(
        state_cache,
        first_step_probe,
        first_step_address,
        first_step_content,
        first_step_outgate,
        first_step_strength_raw,
        channel_scaling_factor,
    )
    group_terms = jnp.dot(
        heads_read, readout_projection, preferred_element_type=jnp.float32
    ).astype(jnp.bfloat16)
    return (state_cache, lax.psum(group_terms, "tp"), boundary_cache)


def by_heads(mesh):
    def choose(*args):
        seq_count, length, model_width = args[0].shape
        peers, heads = lax.axis_size("sp"), args[6].shape[0]
        fits = (
            lax.axis_size("tp") == 2
            and seq_count == 2
            and peers == 2 * heads
            and heads % 2 == 0
            and length == BLOCK
            and args[1].shape[0] * peers == model_width
        )
        return per_device_heads(*args) if fits else per_device(*args)

    return choose


def solution(mesh):
    return jax.shard_map(
        by_heads(mesh),
        mesh=mesh,
        in_specs=(
            P(None, "sp", None),
            P("sp", "tp"),
            P("sp", "tp"),
            P(),
            P(),
            P("tp"),
            P("tp"),
            P(None, "sp", "tp"),
            P(None, "tp"),
            P(None, "tp"),
            P(None, "tp"),
            P(None, "tp"),
            P(None, "tp"),
            P(),
            P("tp", "sp"),
        ),
        out_specs=(P(None, "tp", None, None), P(None, "sp"), P(None, "sp", "tp", None, None)),
        check_vma=False,
    )
```

profile of v0, /device:TPU:9, one launch (start us, length us, event | category | flops | bytes accessed | tf_op | source)
XLA Modules:
  0.0 136.4 jit_solution(11826619893871027325)
XLA Ops:
  0.7 0.9 fusion.44
  1.6 0.3 copy.34
  1.9 0.9 pad.8.refs_4_
  2.8 78.9 %gather_inputs.1 = (bf16[16,64,384]{2,1,0:T(8,128)(2,1)}, f32[16,8,64]{2,1,0:T(8,128)}) custom-call(bf16[2,64,4096]{2,1,0:T(8,128)(2,1)} %refs_0_.1, bf16[256,1024]{1,0:T(8,128)(2,1)} %refs_1_.1, bf16[256,1024]{1,0:T(8,128)(2,1)} %refs_2_.1, f32[2,8,64]{2,1,0:T(8,128)} %bitcast.82, bf16[2048,128]{1,0:T(8,128)(2,1)} %pad.8.refs_4_), custom_call_target="tpu_custom_call" | custom-call | tf_op jit(solution)/shard_map/gather_inputs/pallas_call | solution.py:504
  81.7 1.1 slice.114
  82.8 0.5 constant_dynamic-slice_fusion
  83.3 0.9 constant_dynamic-slice_fusion.1
  84.2 0.6 dynamic_slice.22
  84.8 0.7 fusion.60
  85.5 0.2 reduce_window_sum.11
  85.7 0.2 slice_reduce_fusion
  85.9 0.2 convert_element_type.54
  86.0 0.3 divide_multiply_fusion
  86.3 0.2 multiply_reduce_fusion
  86.6 0.2 copy.36
  86.8 0.6 dynamic_slice.25
  87.4 0.7 divide_reduce_fusion
  88.2 0.5 multiply_multiply_fusion
  88.7 0.9 fusion.10
  89.5 0.4 fusion.71
  89.9 0.4 fusion.31
  90.3 0.4 fusion.72
  90.7 0.4 fusion.29
  91.1 0.4 fusion.73
  91.4 0.4 fusion.27
  91.8 0.4 fusion.74
  92.2 0.4 fusion.25
  92.5 0.4 convolution_add_fusion.1
  92.9 0.4 fusion.75
  93.3 0.6 fusion.11
  93.8 1.4 %fusion.34 = f32[16,128,256]{2,1,0:T(8,128)S(1)} fusion(f32[16,64,256]{2,1,0:T(8,128)S(1)} %fusion.11, f32[16,64,256]{2,1,0:T(8,128)S(1)} %divide_multiply_fusion, f32[16,64]{1,0:T(8,128)S(1)} %get-tuple-element.30, f32[16,64]{1,0:T(8,128)S(1)} %get-tuple-element.32), kind=kOutput, calls=%fused_computation.52 | convolution fusion | flops 201588736 | bytes 3686400 | tf_op jit(solution)/shard_map/nck,ncj->nkj/dot_general | solution.py:604
  95.3 0.2 fusion.70
  95.6 1.0 pad_add_fusion
  96.7 0.2 fusion
  97.0 1.1 pad_add_fusion.1
  98.1 0.9 pad_add_fusion.2
  99.1 0.4 fusion.69
  99.5 0.7 fusion.9
  100.2 0.9 pad_maximum_fusion.10.refs_0_
  101.1 21.4 %spread_states.1 = (bf16[16,128,128]{2,1,0:T(8,128)(2,1)}, bf16[16,128,128]{2,1,0:T(8,128)(2,1)}) custom-call(bf16[16,128,128]{2,1,0:T(8,128)(2,1)} %pad_maximum_fusion.10.refs_0_), custom_call_target="tpu_custom_call" | custom-call | tf_op jit(solution)/shard_map/spread_states/pallas_call | solution.py:592
  122.6 0.1 fusion.62
  122.8 1.6 %fusion.76 = f32[2,8,1,128]{3,2,1,0:T(1,128)S(1)} fusion(f32[2,8,128,1]{2,3,1,0:T(1,128)S(1)} %bitcast.78, bf16[2,8,128,128]{3,2,1,0:T(8,128)(2,1)} %bitcast.73), kind=kOutput, calls=%fused_computation.127 | convolution fusion | flops 3145728 | bytes 540672 | tf_op jit(solution)/shard_map/nhk,nhkv->nhv/dot_general | solution.py:174
  124.5 2.2 %fusion.15 = f32[2,8,1,128]{3,2,1,0:T(1,128)S(1)} fusion(f32[2,8,128,1]{2,3,1,0:T(1,128)S(1)} %bitcast.83, bf16[2,8,128,128]{3,2,1,0:T(8,128)(2,1)} %bitcast.74, f32[2,8,128]{2,1,0:T(8,128)S(1)} %bitcast_subtract_fusion, f32[2,8,128]{2,1,0:T(8,128)S(1)} %get-tuple-element.20), kind=kOutput, calls=%fused_computation.29 | convolution fusion | flops 3932160 | bytes 557056 | tf_op jit(solution)/shard_map/nhk,nhkv->nhv/dot_general | solution.py:183
  126.7 0.1 multiply_reduce_fusion.1
  126.9 0.2 convolution_convert_fusion
  127.1 7.7 %psum.7 = bf16[2,256]{1,0:T(2,128)(2,1)} all-reduce(bf16[2,256]{1,0:T(2,128)(2,1)S(1)} %convolution_convert_fusion), channel_id=1, replica_groups=mesh['sp'=16,'tp'=2] {'tp'}, use_global_device_ids=true, to_apply=%region_4.5 | all-reduce | flops 512 | bytes 2048 | tf_op jit(solution)/shard_map/psum | solution.py:717
  134.8 0.8 copy.58
  135.6 0.8 copy.59
  (46 shorter events, 0.8 us)
Async XLA Ops:
  0.6 126.3 %copy-start = (bf16[1024,256]{1,0:T(8,128)(2,1)S(1)}, bf16[1024,256]{1,0:T(8,128)(2,1)}, u32[]{:S(2)}) copy-start(bf16[1024,256]{1,0:T(8,128)(2,1)} %param.29) | copy-start | bytes 1572868
  81.7 2.5 %copy-start.10 = (f32[8]{0:T(128)S(1)}, f32[8]{0:T(128)}, u32[]{:S(2)}) copy-start(f32[8]{0:T(128)} %param.21) | copy-start | bytes 100
  81.7 4.2 %copy-start.1 = (bf16[16,64,384]{2,1,0:T(8,128)(2,1)S(1)}, bf16[16,64,384]{2,1,0:T(8,128)(2,1)}, u32[]{:S(2)}) copy-start(bf16[16,64,384]{2,1,0:T(8,128)(2,1)} %get-tuple-element.8) | copy-start | bytes 2359300
  86.0 0.8 copy-start.11
  99.5 23.1 %copy-start.4 = (bf16[2,1024]{1,0:T(2,128)(2,1)S(1)}, bf16[2,1024]{1,0:T(2,128)(2,1)}, u32[]{:S(2)}) copy-start(bf16[2,1024]{1,0:T(2,128)(2,1)} %param.24) | copy-start | bytes 12292
  99.5 23.2 %copy-start.8 = (f32[2,8]{1,0:T(2,128)S(1)}, f32[2,8]{1,0:T(2,128)}, u32[]{:S(2)}) copy-start(f32[2,8]{1,0:T(2,128)} %param.27) | copy-start | bytes 196
  100.2 24.3 %copy-start.5 = (bf16[2,1024]{1,0:T(2,128)(2,1)S(1)}, bf16[2,1024]{1,0:T(2,128)(2,1)}, u32[]{:S(2)}) copy-start(bf16[2,1024]{1,0:T(2,128)(2,1)} %param.25) | copy-start | bytes 12292
  100.2 24.3 %copy-start.6 = (bf16[2,1024]{1,0:T(2,128)(2,1)S(1)}, bf16[2,1024]{1,0:T(2,128)(2,1)}, u32[]{:S(2)}) copy-start(bf16[2,1024]{1,0:T(2,128)(2,1)} %param.23) | copy-start | bytes 12292
  100.2 26.6 %copy-start.7 = (bf16[2,1024]{1,0:T(2,128)(2,1)S(1)}, bf16[2,1024]{1,0:T(2,128)(2,1)}, u32[]{:S(2)}) copy-start(bf16[2,1024]{1,0:T(2,128)(2,1)} %param.26) | copy-start | bytes 12292
  100.2 26.6 %copy-start.9 = (f32[128]{0:T(128)S(1)}, f32[128]{0:T(128)}, u32[]{:S(2)}) copy-start(f32[128]{0:T(128)} %param.28) | copy-start | bytes 1540
  122.6 12.2 %copy-start.2 = (bf16[16,128,128]{2,1,0:T(8,128)(2,1)S(1)}, bf16[16,128,128]{2,1,0:T(8,128)(2,1)}, u32[]{:S(2)}) copy-start(bf16[16,128,128]{2,1,0:T(8,128)(2,1)} %get-tuple-element.9) | copy-start | bytes 1572868
  122.6 13.0 %copy-start.3 = (bf16[16,128,128]{2,1,0:T(8,128)(2,1)S(1)}, bf16[16,128,128]{2,1,0:T(8,128)(2,1)}, u32[]{:S(2)}) copy-start(bf16[16,128,128]{2,1,0:T(8,128)(2,1)} %get-tuple-element.10) | copy-start | bytes 1572868
where the time goes:
time: 137 us; the launch traced here: 136 us
  Pallas kernels  100 us (73%)
  matrix products  14.2 us (10%)
  blocking collectives  7.67 us (6%)
  local copies, waits for them, and re-layouts  7.2 us (5%)
  other arithmetic  5.88 us (4%)
    pallas_call x1, Pallas kernels, gather_inputs(): pl.pallas_call(lambda *refs: gather_kernel(peers, *refs), out_shape=(jax....  78.9 us
    pallas_call x1, Pallas kernels, spread_states(): pl.pallas_call(lambda *refs: spread_kernel(peers, *refs), out_shape=(jax....  21.4 us
    dot_general x17, matrix products, dot32(): return jnp.einsum(spec, a, b, precision=lax.Precision.HIGH)  10.2 us
    psum x1, blocking collectives, per_device_heads(): return (state_cache, lax.psum(group_terms, 'tp'), boundary_cache)  7.67 us

commit v1 on v0

v1 whole, which is shorter than its diff:
```python
import jax
import jax.numpy as jnp
from jax import lax
from jax.experimental import pallas as pl
from jax.experimental.pallas import tpu as pltpu
from jax.sharding import PartitionSpec as P

ADDRESS_WIDTH = 128
BLOCK = 64


EPSILON = 1e-06
HIGHEST_ACCURACY = lax.Precision.HIGHEST


def prefix(array, axis, combine, identity):
    peers, index = (lax.axis_size(axis), lax.axis_index(axis))
    everything = jax.tree.map(
        lambda part, kind: lax.all_gather(part.astype(kind), axis),
        array,
        (jnp.bfloat16, jnp.bfloat16),
    )
    start = jax.tree.map(
        lambda part, zero: jnp.broadcast_to(jnp.asarray(zero, part.dtype), part.shape),
        array,
        identity,
    )

    def step(k, before):
        reached = k < index
        new = combine(
            before, jax.tree.map(lambda part, own: part[k].astype(own.dtype), everything, array)
        )
        return jax.tree.map(lambda a, b: jnp.where(reached, a, b), new, before)

    return lax.fori_loop(0, peers, step, start)


def as_sent(array):
    return jax.tree.map(lambda a: a.astype(jnp.bfloat16) if a.dtype == jnp.float32 else a, array)


def broadcast(value, axis, source):
    kept = jnp.where(lax.axis_index(axis) == source, value, 0).astype(value.dtype)
    return lax.psum(kept, axis)


def unit_inverse(lower_part):
    matrix_order = lower_part.shape[-1]
    identity = jnp.eye(matrix_order, dtype=jnp.float32)
    result = identity - lower_part
    power_term = lower_part
    reached = 2
    while reached < matrix_order:
        power_term = jnp.matmul(power_term, power_term, precision=HIGHEST_ACCURACY)
        result = jnp.matmul(result, identity + power_term, precision=HIGHEST_ACCURACY)
        reached = reached * 2
    return result


def build_arguments(
    address_vectors,
    content_vectors,
    outgate_raw_scores,
    strength_offset,
    channel_fading_speed,
    added_fading_exponent,
    channel_width,
):
    length = address_vectors.shape[0]
    attention_channels_total = channel_fading_speed.shape[0]
    address_token_slab = jax.nn.silu(address_vectors.astype(jnp.float32)).reshape(
        length, attention_channels_total, channel_width
    )
    address_token_slab = address_token_slab * lax.rsqrt(
        jnp.sum(address_token_slab * address_token_slab, axis=-1, keepdims=True) + EPSILON
    )
    content_token_slab = jax.nn.silu(content_vectors.astype(jnp.float32)).reshape(
        length, attention_channels_total, channel_width
    )
    strength_raw_expanded = outgate_raw_scores.astype(jnp.float32)
    storing_strength = jax.nn.sigmoid(
        strength_raw_expanded[:, :attention_channels_total] + strength_offset
    )
    fading_exponent = added_fading_exponent - channel_fading_speed * jax.nn.softplus(
        strength_raw_expanded[:, attention_channels_total:]
    )
    return (address_token_slab, content_token_slab, storing_strength, fading_exponent)


def range_map(address_token_slab, content_token_slab, storing_strength, fading_exponent, block):
    length, attention_channels_total, channel_width = address_token_slab.shape
    blocks = length // block

    def split_blocks(tensor):
        moved_axes = jnp.swapaxes(tensor, 0, 1)
        return moved_axes.reshape((attention_channels_total, blocks, block) + moved_axes.shape[2:])

    block_keys = split_blocks(address_token_slab)
    block_values = split_blocks(content_token_slab)
    block_beta = split_blocks(storing_strength)
    cumulative = jnp.cumsum(split_blocks(fading_exponent), axis=-1)
    positions = jnp.arange(block)
    strict = positions[:, None] > positions[None, :]
    spread_log = jnp.where(strict, cumulative[..., :, None] - cumulative[..., None, :], 0.0)
    scaled_keys = block_keys * block_beta[..., None]
    inner_prod = jnp.einsum("hnik,hnjk->hnij", scaled_keys, block_keys, precision=HIGHEST_ACCURACY)
    lower_part = jnp.where(strict, inner_prod * jnp.exp(spread_log), 0.0)
    inverse = unit_inverse(lower_part)
    targets = jnp.concatenate(
        [block_values * block_beta[..., None], scaled_keys * jnp.exp(cumulative)[..., None]],
        axis=-1,
    )
    solved = jnp.einsum("hnij,hnjk->hnik", inverse, targets, precision=HIGHEST_ACCURACY)
    updates = solved[..., :channel_width]
    key_weights = solved[..., channel_width:]
    tail_keys = block_keys * jnp.exp(cumulative[..., -1:] - cumulative)[..., None]
    last_decay = jnp.exp(cumulative[..., -1])
    identity = jnp.eye(channel_width, dtype=jnp.float32)

    def advance(state_pair, block_items):
        transition, carried_state = state_pair
        update_index, weight_index, tail_index, last_index = block_items
        fresh_value_rows = update_index - jnp.einsum(
            "xbg,xgp->xbp", weight_index, carried_state, precision=HIGHEST_ACCURACY
        )
        carried_state = carried_state * last_index[:, None, None] + jnp.einsum(
            "tjo,tjw->tow", tail_index, fresh_value_rows, precision=HIGHEST_ACCURACY
        )
        block_move = last_index[:, None, None] * identity - jnp.einsum(
            "hck,hcj->hkj", tail_index, weight_index, precision=HIGHEST_ACCURACY
        )
        transition = jnp.einsum("hij,hjk->hik", block_move, transition, precision=HIGHEST_ACCURACY)
        return ((transition, carried_state), None)

    initial = (
        jnp.broadcast_to(identity, (attention_channels_total, channel_width, channel_width)),
        jnp.zeros((attention_channels_total, channel_width, channel_width), jnp.float32),
    )
    block_items = (
        jnp.moveaxis(updates, 1, 0),
        jnp.moveaxis(key_weights, 1, 0),
        jnp.moveaxis(tail_keys, 1, 0),
        jnp.moveaxis(last_decay, 1, 0),
    )
    (transition, carried_state), _ = lax.scan(advance, initial, block_items)
    return (transition, carried_state)


def read_heads(
    state_cache,
    first_step_probe,
    first_step_address,
    first_step_content,
    first_step_outgate,
    first_step_strength_raw,
    channel_scaling_factor,
):
    seq_count, attention_channels_total, channel_width, _ = state_cache.shape
    carried_state = state_cache.astype(jnp.float32)

    def activate(tensor):
        return jax.nn.silu(tensor.astype(jnp.float32)).reshape(
            seq_count, attention_channels_total, channel_width
        )

    query_rows = activate(first_step_probe)
    address_token_slab = activate(first_step_address)
    address_token_slab = address_token_slab * lax.rsqrt(
        jnp.sum(address_token_slab * address_token_slab, axis=-1, keepdims=True) + EPSILON
    )
    content_token_slab = activate(first_step_content)
    storing_strength = jax.nn.sigmoid(first_step_strength_raw)
    recalled = jnp.einsum(
        "nhk,nhkv->nhv", address_token_slab, carried_state, precision=HIGHEST_ACCURACY
    )
    updated = (
        carried_state
        + storing_strength[..., None, None]
        * address_token_slab[..., :, None]
        * (content_token_slab - recalled)[..., None, :]
    )
    output = jnp.einsum("nhk,nhkv->nhv", query_rows, updated, precision=HIGHEST_ACCURACY)
    normed = (
        output
        * lax.rsqrt(jnp.mean(output * output, axis=-1, keepdims=True) + EPSILON)
        * channel_scaling_factor
    )
    gated_out = normed * activate(first_step_outgate)
    return gated_out.reshape(seq_count, attention_channels_total * channel_width).astype(
        jnp.bfloat16
    )


def matmul_maps(left, right):
    return jnp.einsum("shij,shjk->shik", left, right, precision=HIGHEST_ACCURACY)


def join_pairs(earlier, later):
    return (matmul_maps(later[0], earlier[0]), matmul_maps(later[0], earlier[1]) + later[1])


def per_device(
    layer_source_tokens,
    address_projection,
    content_projection,
    strength_projection,
    fading_driver_projection,
    strength_offset,
    channel_fading_speed,
    added_fading_exponent,
    first_step_probe,
    first_step_address,
    first_step_content,
    first_step_outgate,
    first_step_strength_raw,
    channel_scaling_factor,
    readout_projection,
):
    head_local = channel_fading_speed.shape[0]
    first_head = lax.axis_index("tp") * head_local
    beta_slice = lax.dynamic_slice_in_dim(strength_projection, first_head, head_local, 1)
    alpha_slice = lax.dynamic_slice_in_dim(fading_driver_projection, first_head, head_local, 1)
    seq_count, local_len, model_width = layer_source_tokens.shape
    flat_rows = layer_source_tokens.reshape(seq_count * local_len, model_width)
    key_sum = jnp.dot(
        flat_rows,
        lax.all_gather(address_projection, "sp", axis=0, tiled=True),
        preferred_element_type=jnp.float32,
    )
    value_sum = jnp.dot(
        flat_rows,
        lax.all_gather(content_projection, "sp", axis=0, tiled=True),
        preferred_element_type=jnp.float32,
    )
    beta_sum = jnp.dot(flat_rows, beta_slice, preferred_element_type=jnp.float32)
    alpha_sum = jnp.dot(flat_rows, alpha_slice, preferred_element_type=jnp.float32)
    outgate_raw_scores = (
        jnp.concatenate([beta_sum, alpha_sum], axis=1)
        .astype(jnp.bfloat16)
        .reshape(seq_count, local_len, -1)
    )
    address_vectors = key_sum.astype(jnp.bfloat16).reshape(seq_count, local_len, -1)
    content_vectors = value_sum.astype(jnp.bfloat16).reshape(seq_count, local_len, -1)
    transitions = []
    offsets = []
    for prompt_number in range(seq_count):
        address_token_slab, content_token_slab, storing_strength, fading_exponent = build_arguments(
            address_vectors[prompt_number],
            content_vectors[prompt_number],
            outgate_raw_scores[prompt_number],
            strength_offset,
            channel_fading_speed,
            added_fading_exponent[prompt_number],
            ADDRESS_WIDTH,
        )
        transition, carried_state = range_map(
            address_token_slab, content_token_slab, storing_strength, fading_exponent, BLOCK
        )
        transitions.append(transition)
        offsets.append(carried_state)
    transition = jnp.stack(transitions)
    offset = jnp.stack(offsets)
    identity = jnp.broadcast_to(jnp.eye(ADDRESS_WIDTH, dtype=jnp.float32), transition.shape)
    entered = prefix((transition, offset), "sp", join_pairs, (identity, jnp.zeros_like(offset)))
    leaving = matmul_maps(transition, entered[1]) + offset
    final = broadcast(as_sent(leaving), "sp", lax.axis_size("sp") - 1).astype(leaving.dtype)
    boundary_cache = leaving.astype(jnp.bfloat16)[:, None]
    state_cache = final.astype(jnp.bfloat16)
    heads_read = read_heads(
        state_cache,
        first_step_probe,
        first_step_address,
        first_step_content,
        first_step_outgate,
        first_step_strength_raw,
        channel_scaling_factor,
    )
    group_terms = jnp.dot(
        heads_read, readout_projection, preferred_element_type=jnp.float32
    ).astype(jnp.bfloat16)
    mixed_read = lax.psum(group_terms.astype(jnp.float32).astype(jnp.bfloat16), "tp")
    return (state_cache, mixed_read, boundary_cache)


MESH = pl.DeviceIdType.MESH
PIECES = 2
DEEP = 4
PLANE = 4


def remote(src, dst, send, recv, sp, tp):
    return pltpu.make_async_remote_copy(
        src_ref=src,
        dst_ref=dst,
        send_sem=send,
        recv_sem=recv,
        device_id={"sp": sp, "tp": tp},
        device_id_type=MESH,
    )


def silu(v):
    return v / (1.0 + jnp.exp(-v))


def sigmoid(v):
    return 1.0 / (1.0 + jnp.exp(-v))


def softplus(v):
    return jnp.maximum(v, 0.0) + jnp.log1p(jnp.exp(-jnp.abs(v)))


def halves(a):
    high = a.astype(jnp.bfloat16)
    return high, (a - high.astype(jnp.float32)).astype(jnp.bfloat16)


NN = (((1,), (0,)), ((), ()))
NT = (((1,), (1,)), ((), ()))
TN = (((0,), (0,)), ((), ()))


def dot3(a, b, dims=NN):
    def one(p, q):
        return lax.dot_general(p, q, dims, preferred_element_type=jnp.float32)

    (ah, al), (bh, bl) = a, b
    return one(ah, bh) + (one(ah, bl) + one(al, bh))


def choose(table, index):
    value = jnp.int32(table[0])
    for at in range(1, len(table)):
        value = jnp.where(index == at, jnp.int32(table[at]), value)
    return value


def by_distance(k):
    order = []
    for z in range(DEEP):
        others = sorted((abs(o - z), o) for o in range(DEEP) if o != z)
        order.append(others[k - 1][1])
    return order


def prefill_kernel(
    peers,
    tok,
    wk,
    wv,
    gate_b,
    gate_a,
    add,
    offset,
    speed,
    probe,
    address,
    content,
    outgate,
    strength,
    gain,
    readout,
    final,
    bound,
    mixed,
    xall,
    wall,
    wcross,
    tokv,
    gatev,
    addv,
    logit,
    msg,
    gall,
    keep,
    give,
    got,
    pair,
    states,
    rv,
    rmsg,
    rall,
    part,
    partgot,
    load,
    own_sem,
    z_send,
    tok_recv,
    x_send,
    y_send,
    xf_send,
    yf_send,
    w_send,
    w_recv,
    c_recv,
    relay_send,
    cross_send,
    outer_send,
    blk_recv,
    g_send,
    g_recv,
    give_send,
    give_recv,
    f_send,
    f_recv,
    b_send,
    b_recv,
    r_send,
    r_recv,
    t_send,
    t_recv,
):
    s, t = lax.axis_index("sp"), lax.axis_index("tp")
    heads = add.shape[1]
    width = ADDRESS_WIDTH
    length = tok.shape[1]
    half = tok.shape[2] // 2
    rows = wk.shape[0]
    piece = length // PIECES
    x, y, z = s % 2, (s // 2) % 2, s // PLANE
    prompt, side = z % 2, z // 2
    j = side * PLANE + s % PLANE
    mate = z + 1 - 2 * prompt
    columns = pl.ds(pl.multiple_of(t * half, 128), half)

    def chip(cx, cy, cz):
        return PLANE * cz + 2 * cy + cx

    def slot_of(c):
        return (c // PLANE % 2) * heads + (c // PLANE // 2) * PLANE + c % PLANE

    x_peer, y_peer, z_peer = chip(1 - x, y, z), chip(x, 1 - y, z), chip(x, y, mate)
    diagonal = chip(1 - x, 1 - y, z)
    home = t == side

    def part_of(i):
        return pl.ds(i * piece, piece)

    sent = []

    def go(copy):
        copy.start()
        sent.append(copy)

    def token_wait(c, i):
        ref = xall.at[c, part_of(i)]
        remote(ref, ref, own_sem, tok_recv.at[c, i], s, t).wait_recv()

    loads = []
    for i, (src, dst) in enumerate(
        (
            (tok, tokv),
            (gate_b, gatev.at[0]),
            (gate_a, gatev.at[1]),
            (add, addv),
            (readout, rv),
        )
    ):
        copy = pltpu.make_async_copy(src, dst, load.at[i])
        copy.start()
        loads.append(copy)

    near = [z] + [choose(by_distance(k), z) for k in range(1, DEEP)]
    for k in range(1, DEEP):
        for i in range(PIECES):
            go(
                remote(
                    tok.at[near[k] % 2, part_of(i), columns],
                    xall.at[s, part_of(i)],
                    z_send.at[k, i],
                    tok_recv.at[s, i],
                    chip(x, y, near[k]),
                    t,
                )
            )
    own = pltpu.make_async_copy(tok.at[prompt, :, columns], xall.at[s], own_sem)
    own.start()

    side_of = (t + side) % 2
    own_row = s % (peers // 2)
    q_own = s % PLANE
    spot = pl.ds(pl.multiple_of(own_row * rows, 16), rows)

    def weight_copies(dx, dy, cross, kv):
        xd, yd = (x + dx) % 2, (y + dy) % 2
        head = ((side + cross) % 2) * PLANE + 2 * yd + xd
        src = (wk, wv)[kv].at[:, pl.ds(pl.multiple_of(head * width, 128), width)]
        at = pl.ds(pl.multiple_of((2 * side_of + kv) * width, 128), width)
        if cross:
            dst, sem = wcross.at[q_own, :, at], c_recv.at[q_own, 2 * side_of + kv]
        else:
            dst, sem = wall.at[spot, at], w_recv.at[own_row, 2 * side_of + kv]
        out = w_send.at[2 * dy + dx, 2 * cross + kv]
        return src, dst, sem, remote(src, dst, out, sem, chip(xd, yd, z), side)

    for dx, dy in ((0, 0), (1, 0), (0, 1), (1, 1)):
        for cross in (1, 0):
            for kv in range(2):
                src, dst, sem, copy = weight_copies(dx, dy, cross, kv)
                if dx + dy == 0:

                    @pl.when(home)
                    def _():
                        pltpu.make_async_copy(src, dst, sem).start()

                    @pl.when(jnp.logical_not(home))
                    def _():
                        copy.start()
                else:
                    go(copy)

    for i in range(PIECES):
        src = tok.at[prompt, part_of(i), columns]
        dst = xall.at[s, part_of(i)]
        go(remote(src, dst, x_send.at[0, i], tok_recv.at[s, i], x_peer, t))
        go(remote(src, dst, y_send.at[0, i], tok_recv.at[s, i], y_peer, t))

    loads[0].wait()
    loads[1].wait()
    loads[2].wait()
    loads[3].wait()
    total_heads = gate_b.shape[0]
    msg[...] = jnp.zeros_like(msg)
    for p in range(2):
        for kind in range(2):
            logit[p, kind] = (
                lax.dot_general(gatev[kind], tokv[p], NT, preferred_element_type=jnp.float32)
                .astype(jnp.bfloat16)
                .astype(jnp.float32)
            )
        for h in range(heads):
            for kind in range(2):
                msg[p, h, kind : kind + 1, :] = logit[p, kind, pl.ds(t * heads + h, 1), :]
            msg[p, h, 2:3, :] = addv[p, h : h + 1, :]
    for off in range(1, peers):
        to = (s + off) % peers
        to_z = to // PLANE
        go(
            remote(
                msg.at[to_z % 2, (to_z // 2) * PLANE + to % PLANE],
                gall.at[s],
                g_send.at[off],
                g_recv.at[s],
                to,
                t,
            )
        )
    gall[s] = msg[prompt, j]

    def home_relay(dx, dy):
        q = 2 * ((y + dy) % 2) + (x + dx) % 2
        row = prompt * PLANE + q
        block = wall.at[pl.ds(pl.multiple_of(row * rows, 16), rows)]
        landing = chip(x, y, DEEP // 2 - side)
        for c in range(4):
            one = wcross.at[q, :, pl.ds(c * width, width)]
            pltpu.make_async_copy(one, one, c_recv.at[q, c]).wait()
        remote(
            wcross.at[q], block, cross_send.at[q], blk_recv.at[row], landing, t
        ).start()
        for c in range(4):
            one = wall.at[
                pl.ds(pl.multiple_of(row * rows, 16), rows), pl.ds(c * width, width)
            ]
            pltpu.make_async_copy(one, one, w_recv.at[row, c]).wait()
        remote(block, block, relay_send.at[q], blk_recv.at[row], z_peer, t).start()

    inner = prompt != side
    lands = jnp.logical_and(jnp.logical_not(home), inner)

    def block_of(row):
        return wall.at[pl.ds(pl.multiple_of(row * rows, 16), rows)]

    def land_relay(n):
        row = arrival_row(n)
        ref = block_of(row)
        remote(ref, ref, outer_send.at[n], blk_recv.at[row], s, t).wait_recv()
        remote(ref, ref, outer_send.at[n], blk_recv.at[row], z_peer, t).start()

    def arrival_row(n):
        plane = (side + n) % 2
        step = n // 2
        q = 2 * ((y + step // 2) % 2) + (x + step % 2) % 2
        return plane * PLANE + q

    def on_home(dx, dy):
        @pl.when(home)
        def _():
            home_relay(dx, dy)

    def on_land(ns):
        @pl.when(lands)
        def _():
            for n in ns:
                land_relay(n)

    def spread_column(k):
        for i in range(PIECES):
            c = chip(x, y, near[k])
            token_wait(c, i)
            ref = xall.at[c, part_of(i)]
            go(remote(ref, ref, x_send.at[k, i], tok_recv.at[c, i], x_peer, t))
            go(remote(ref, ref, y_send.at[k, i], tok_recv.at[c, i], y_peer, t))

    def cross_plane(k):
        c = chip(1 - x, y, near[k])
        token_wait(c, 0)
        ref = xall.at[c, part_of(0)]
        go(remote(ref, ref, yf_send.at[k], tok_recv.at[c, 0], y_peer, t))
        c = chip(x, 1 - y, near[k])
        token_wait(c, 1)
        ref = xall.at[c, part_of(1)]
        go(remote(ref, ref, xf_send.at[k], tok_recv.at[c, 1], x_peer, t))

    on_home(0, 0)
    on_home(1, 0)
    on_home(0, 1)
    spread_column(1)
    on_home(1, 1)
    cross_plane(0)
    on_land((0, 1))
    spread_column(2)
    cross_plane(1)
    on_land((2, 3))
    spread_column(3)
    on_land((4, 5))
    cross_plane(2)
    on_land((6, 7))
    cross_plane(3)

    for n in range(PLANE):

        @pl.when(home)
        def _():
            row = (1 - prompt) * PLANE + n
            ref = block_of(row)
            remote(ref, ref, own_sem, blk_recv.at[row], s, t).wait_recv()

    for row in range(2 * PLANE):

        @pl.when(jnp.logical_and(jnp.logical_not(home), jnp.logical_not(inner)))
        def _():
            ref = block_of(row)
            remote(ref, ref, own_sem, blk_recv.at[row], s, t).wait_recv()

    own.wait()
    for off in range(1, peers):
        c = (s + off) % peers
        remote(gall.at[c], gall.at[c], own_sem, g_recv.at[c], s, t).wait_recv()

    def slots_of(g):
        cx, cy = (x + g % 2) % 2, (y + g // 2) % 2
        return [chip(cx, cy, k) for k in range(DEEP)]

    def exchange(c):
        return remote(give.at[c], got.at[c], give_send.at[c], give_recv.at[c], s, 1 - t)

    def project(g):
        slots = slots_of(g)

        @pl.when(g % 2 == 1)
        def _():
            for c in slots:
                token_wait(c, 1)

        @pl.when(g // 2 == 1)
        def _():
            for c in slots:
                token_wait(c, 0)

        rows_in = jnp.concatenate([xall[c] for c in slots], axis=0)
        wide = jnp.dot(rows_in, wall[...], preferred_element_type=jnp.float32)
        for i, c in enumerate(slots):
            part_rows = slice(i * length, (i + 1) * length)
            keep[c] = wide[part_rows, : 2 * width]
            give[c] = wide[part_rows, 2 * width :]
        for c in slots:
            exchange(c).start()

    many = DEEP * length

    def local(g):
        slots = slots_of(g)
        for c in slots:
            exchange(c).wait_recv()
        wide = jnp.concatenate([keep[c] + got[c] for c in slots], axis=0)
        acted = silu(wide.astype(jnp.bfloat16).astype(jnp.float32))
        k = acted[:, :width]
        k = k * lax.rsqrt(jnp.sum(k * k, axis=-1, keepdims=True) + EPSILON)
        v = acted[:, width:]

        def row_of(kind):
            return jnp.concatenate([gall[c, kind : kind + 1, :] for c in slots], axis=1)

        beta_row = sigmoid(row_of(0) + offset[j])
        fade_row = row_of(2) - speed[j] * softplus(row_of(1))
        r = lax.broadcasted_iota(jnp.int32, (many, many), 0)
        c = lax.broadcasted_iota(jnp.int32, (many, many), 1)
        same = r // length == c // length
        strict = jnp.logical_and(same, r > c)
        eye = r == c

        def column(mask, row):
            return jnp.sum(jnp.where(mask, row, 0.0), axis=1, keepdims=True)

        sum_col = column(jnp.logical_and(same, r >= c), fade_row)
        all_col = column(same, fade_row)
        beta_col = column(eye, beta_row)
        sum_row = jnp.sum(jnp.where(eye, sum_col, 0.0), axis=0, keepdims=True)
        scaled = k * beta_col
        inner_products = dot3(halves(scaled), halves(k), NT)
        spread = jnp.exp(jnp.where(strict, sum_col - sum_row, 0.0))
        power = halves(jnp.where(strict, inner_products * spread, 0.0))
        solved = jnp.concatenate([scaled * jnp.exp(sum_col), v * beta_col], axis=1)
        solved = solved - dot3(power, halves(solved))
        reached = 2
        while reached < length:
            power = halves(dot3(power, power))
            solved = solved + dot3(power, halves(solved))
            reached *= 2
        tail = halves(k * jnp.exp(all_col - sum_col))
        solved = halves(solved)
        unit = (
            lax.broadcasted_iota(jnp.int32, (width, width), 0)
            == lax.broadcasted_iota(jnp.int32, (width, width), 1)
        ).astype(jnp.float32)
        last = jnp.exp(all_col)
        for i, slot in enumerate(slots):
            at = slice(i * length, (i + 1) * length)
            maps = dot3(
                tuple(a[at] for a in tail), tuple(a[at] for a in solved), TN
            )
            moves = last[i * length : i * length + 1] * unit - maps[:, :width]
            pair[slot, :, :width] = moves
            pair[slot, :, width:] = maps[:, width:]

    groups = peers // DEEP

    def stage(g, carry):
        @pl.when(g < groups)
        def _():
            project(g)

        @pl.when(g > 0)
        def _():
            local(g - 1)

        return carry

    lax.fori_loop(0, groups + 1, stage, 0)

    chains = []
    for g in range(groups):
        first = pair[g * DEEP]
        chain = [(first[:, :width], first[:, width:])]
        for i in range(1, DEEP):
            late = pair[g * DEEP + i]
            before = jnp.concatenate(chain[-1], axis=1)
            joined = dot3(halves(late[:, :width]), halves(before))
            chain.append((joined[:, :width], joined[:, width:] + late[:, width:]))
        chains.append(chain)
    carry = None
    found = {}
    for g in range(groups):
        move, shift = chains[g][-1]
        if carry is not None:
            move = halves(move)
            shift = dot3(move, carry[0]) + shift
        found[g * DEEP + DEEP - 1] = shift
        for i in range(DEEP - 1):
            found_shift = chains[g][i][1]
            if carry is not None:
                found_shift = dot3(halves(chains[g][i][0]), carry[0]) + found_shift
            found[g * DEEP + i] = found_shift
        carry = (halves(shift),)
    slot = slot_of(s)
    end = found[peers - 1].astype(jnp.bfloat16)
    final[slot] = end
    f_sent = [0]

    def pass_on(slot_at, to):
        n = f_sent[0]
        f_sent[0] += 1
        ref = final.at[slot_at]
        go(remote(ref, ref, f_send.at[n], f_recv.at[slot_at], to, t))

    def arrived(slot_at):
        ref = final.at[slot_at]
        remote(ref, ref, own_sem, f_recv.at[slot_at], s, t).wait_recv()

    def own_row_of(ref):
        two = ref[:, pl.ds(pl.multiple_of(j * width, 128), width)].astype(jnp.float32)
        return jnp.where(prompt == 0, two[0:1], two[1:2])

    q1 = silu(own_row_of(probe))
    k1 = silu(own_row_of(address))
    k1 = k1 * lax.rsqrt(jnp.sum(k1 * k1, axis=-1, keepdims=True) + EPSILON)
    v1 = silu(own_row_of(content))
    b1 = sigmoid(jnp.full((1, width), strength[prompt, j], jnp.float32))
    q_and_k = jnp.concatenate([q1, k1, jnp.zeros((6, width), jnp.float32)], axis=0)
    recalled = jnp.dot(
        q_and_k,
        end.astype(jnp.float32),
        precision=HIGHEST_ACCURACY,
        preferred_element_type=jnp.float32,
    )
    weight = b1 * jnp.sum(q1 * k1, axis=-1, keepdims=True)
    read = recalled[0:1] + weight * (v1 - recalled[1:2])
    normed = read * lax.rsqrt(jnp.mean(read * read, axis=-1, keepdims=True) + EPSILON)
    gated = normed * gain[...] * silu(own_row_of(outgate))
    rmsg[...] = jnp.broadcast_to(gated.astype(jnp.bfloat16).astype(jnp.float32), rmsg.shape)
    for off in range(1, peers):
        to = (s + off) % peers
        go(remote(rmsg, rall.at[slot], r_send.at[off], r_recv.at[slot], to, t))
    rall[slot] = rmsg[...]

    others = [near[k] for k in range(1, DEEP)]
    for cz in others:
        pass_on(slot, chip(x, y, cz))
    pass_on(slot, y_peer)
    pass_on(slot, x_peer)
    for n in range(peers):
        states[n] = found[n].astype(jnp.bfloat16)
    for off in range(1, peers):
        to = (s + off) % peers
        go(remote(states.at[to], bound.at[slot], b_send.at[off], b_recv.at[slot], to, t))
    bound[slot] = states[s]
    for cz in others:
        come = slot_of(chip(x, y, cz))
        arrived(come)
        pass_on(come, y_peer)
        pass_on(come, x_peer)
    for cz in near:
        come = slot_of(chip(x, 1 - y, cz))
        arrived(come)
        pass_on(come, x_peer)

    for off in range(1, peers):
        come = slot_of((s + off) % peers)
        remote(rall.at[come], rall.at[come], own_sem, r_recv.at[come], s, t).wait_recv()
    lines = [
        jnp.concatenate([rall[p * heads + h, 0:1, :] for h in range(heads)], axis=1)
        for p in range(2)
    ]
    lines.append(jnp.zeros((6, heads * width), jnp.float32))
    heads_read = jnp.concatenate(lines, axis=0).astype(jnp.bfloat16)
    loads[4].wait()
    terms = jnp.dot(heads_read, rv[...], preferred_element_type=jnp.float32)
    part[...] = terms.astype(jnp.bfloat16).astype(jnp.float32)
    swap = remote(part, partgot, t_send, t_recv, s, 1 - t)
    swap.start()
    swap.wait()
    mixed[...] = (part[...] + partgot[...])[:2].astype(mixed.dtype)

    for cz in range(DEEP):
        for cy in range(2):
            arrived(slot_of(chip(1 - x, cy, cz)))
    for off in range(1, peers):
        come = slot_of((s + off) % peers)
        ref = bound.at[come]
        remote(ref, ref, own_sem, b_recv.at[come], s, t).wait_recv()

    for copy in sent:
        copy.wait_send()

    @pl.when(home)
    def _():
        for q in range(PLANE):
            row = prompt * PLANE + q
            ref = block_of(row)
            remote(wcross.at[q], ref, cross_send.at[q], blk_recv.at[row], s, t).wait_send()
            remote(ref, ref, relay_send.at[q], blk_recv.at[row], s, t).wait_send()

    @pl.when(lands)
    def _():
        for n in range(2 * PLANE):
            ref = block_of(arrival_row(n))
            remote(ref, ref, outer_send.at[n], own_sem, s, t).wait_send()

    @pl.when(jnp.logical_not(home))
    def _():
        for cross in (1, 0):
            for kv in range(2):
                weight_copies(0, 0, cross, kv)[3].wait_send()

    def give_done(c, carry):
        exchange(c).wait_send()
        return carry

    lax.fori_loop(0, peers, give_done, 0)


def prefill(tok, wk, wv, gate_b, gate_a, add, offset, speed, first, strength, gain, readout, peers):
    _, length, model_width = tok.shape
    heads = add.shape[1]
    rows = wk.shape[0]
    width = ADDRESS_WIDTH
    half = model_width // 2
    dma = pltpu.SemaphoreType.DMA
    anywhere = pl.BlockSpec(memory_space=pl.ANY)
    vmem = pl.BlockSpec(memory_space=pltpu.VMEM)
    smem = pl.BlockSpec(memory_space=pltpu.SMEM)
    f32, bf16 = jnp.float32, jnp.bfloat16
    return pl.pallas_call(
        lambda *refs: prefill_kernel(peers, *refs),
        out_shape=(
            jax.ShapeDtypeStruct((peers, width, width), bf16),
            jax.ShapeDtypeStruct((peers, width, width), bf16),
            jax.ShapeDtypeStruct((2, readout.shape[1]), bf16),
        ),
        in_specs=[anywhere] * 6 + [smem] * 2 + [vmem] * 4 + [smem, vmem, anywhere],
        out_specs=(vmem, vmem, vmem),
        scratch_shapes=[
            pltpu.VMEM((peers, length, half), bf16),
            pltpu.VMEM((half, 4 * width), bf16),
            pltpu.VMEM((PLANE, rows, 4 * width), bf16),
            pltpu.VMEM(tok.shape, bf16),
            pltpu.VMEM((2,) + gate_b.shape, bf16),
            pltpu.VMEM(add.shape, f32),
            pltpu.VMEM((2, 2, gate_b.shape[0], length), f32),
            pltpu.VMEM((2, heads, 8, length), f32),
            pltpu.VMEM((peers, 8, length), f32),
            pltpu.VMEM((peers, length, 2 * width), f32),
            pltpu.VMEM((peers, length, 2 * width), f32),
            pltpu.VMEM((peers, length, 2 * width), f32),
            pltpu.VMEM((peers, width, 2 * width), f32),
            pltpu.VMEM((peers, width, width), bf16),
            pltpu.VMEM(readout.shape, bf16),
            pltpu.VMEM((8, width), f32),
            pltpu.VMEM((peers, 8, width), f32),
            pltpu.VMEM((8, readout.shape[1]), f32),
            pltpu.VMEM((8, readout.shape[1]), f32),
            dma((5,)),
            dma(()),
            dma((DEEP, PIECES)),
            dma((peers, PIECES)),
            dma((DEEP, PIECES)),
            dma((DEEP, PIECES)),
            dma((DEEP,)),
            dma((DEEP,)),
            dma((4, 4)),
            dma((2 * PLANE, 4)),
            dma((PLANE, 4)),
            dma((PLANE,)),
            dma((PLANE,)),
            dma((2 * PLANE,)),
            dma((2 * PLANE,)),
            dma((peers,)),
            dma((peers,)),
            dma((peers,)),
            dma((peers,)),
            dma((peers,)),
            dma((peers,)),
            dma((peers,)),
            dma((peers,)),
            dma((peers,)),
            dma((peers,)),
            dma(()),
            dma(()),
        ],
        compiler_params=pltpu.CompilerParams(has_side_effects=True),
        name="prefill",
    )(tok, wk, wv, gate_b, gate_a, add, offset, speed, *first, strength, gain, readout)


def per_device_heads(
    layer_source_tokens,
    address_projection,
    content_projection,
    strength_projection,
    fading_driver_projection,
    strength_offset,
    channel_fading_speed,
    added_fading_exponent,
    first_step_probe,
    first_step_address,
    first_step_content,
    first_step_outgate,
    first_step_strength_raw,
    channel_scaling_factor,
    readout_projection,
):
    peers = lax.axis_size("sp")
    head_local = channel_fading_speed.shape[0]
    width = ADDRESS_WIDTH
    final, bound, mixed = prefill(
        layer_source_tokens,
        address_projection,
        content_projection,
        strength_projection.T,
        fading_driver_projection.T,
        jnp.swapaxes(added_fading_exponent, 1, 2),
        strength_offset,
        channel_fading_speed,
        (first_step_probe, first_step_address, first_step_content, first_step_outgate),
        first_step_strength_raw,
        channel_scaling_factor.reshape(1, width),
        readout_projection,
        peers,
    )
    state_cache = final.reshape(2, head_local, width, width)
    boundary_cache = bound.reshape(2, 1, head_local, width, width)
    return (state_cache, mixed, boundary_cache)


def by_heads(mesh):
    def choose_form(*args):
        seq_count, length, model_width = args[0].shape
        peers, heads = lax.axis_size("sp"), args[6].shape[0]
        fits = (
            lax.axis_size("tp") == 2
            and seq_count == 2
            and peers == DEEP * PLANE
            and heads == 2 * PLANE
            and length == BLOCK
            and args[1].shape[0] * peers == model_width
        )
        return per_device_heads(*args) if fits else per_device(*args)

    return choose_form


def solution(mesh):
    return jax.shard_map(
        by_heads(mesh),
        mesh=mesh,
        in_specs=(
            P(None, "sp", None),
            P("sp", "tp"),
            P("sp", "tp"),
            P(),
            P(),
            P("tp"),
            P("tp"),
            P(None, "sp", "tp"),
            P(None, "tp"),
            P(None, "tp"),
            P(None, "tp"),
            P(None, "tp"),
            P(None, "tp"),
            P(),
            P("tp", "sp"),
        ),
        out_specs=(P(None, "tp", None, None), P(None, "sp"), P(None, "sp", "tp", None, None)),
        check_vma=False,
    )
```

time: 137 us -> 112 us (0.82)
  the two profiles are of different devices: /device:TPU:9 before, /device:TPU:0 now
where the time goes in v1:
time: 112 us
  Pallas kernels  108 us (96%)
  local copies, waits for them, and re-layouts  3.31 us (3%)
    pallas_call x1, Pallas kernels, prefill(): pl.pallas_call(lambda *refs: prefill_kernel(peers, *refs), out_shape=(jax...  108 us
    unnamed x7, local copies, waits for them, and re-layouts  3.31 us

profile of v1, /device:TPU:0, one launch (start us, length us, event | category | flops | bytes accessed | tf_op | source)
XLA Modules:
  0.0 112.1 jit_solution(1461327077887806652)
XLA Ops:
  0.6 108.2 %prefill.1 = (bf16[16,128,128]{2,1,0:T(8,128)(2,1)}, bf16[16,128,128]{2,1,0:T(8,128)(2,1)}, bf16[2,256]{1,0:T(2,128)(2,1)}) custom-call(bf16[2,64,4096]{2,1,0:T(8,128)(2,1)} %refs_0_.1, bf16[256,1024]{1,0:T(8,128)(2,1)} %refs_1_.1, bf16[256,1024]{1,0:T(8,128)(2,1)} %refs_2_.1, bf16[16,4096]{1,0:T(8,128)(2,1)} %bitcast.10, bf16[16,4096]{1,0:T(8,128)(2,1)} %bitcast.11, ...), custom_call_target="tpu_custom_call" | custom-call | tf_op jit(solution)/shard_map/prefill/pallas_call | solution.py:906
  108.8 0.0 copy-start.1
  108.8 0.0 copy-start
  108.8 1.9 %copy.22 = bf16[2,8,128,128]{3,2,1,0:T(8,128)(2,1)} copy(bf16[2,8,128,128]{3,2,1,0:T(8,128)(2,1)} %bitcast.9) | data formatting | bytes 1048576
  110.8 0.0 copy-done.1
  110.8 0.6 copy.23
  111.3 0.0 copy-done
  111.3 0.8 copy.24
Async XLA Ops:
  108.8 2.0 %copy-start.1 = (bf16[2,256]{1,0:T(2,128)(2,1)S(1)}, bf16[2,256]{1,0:T(2,128)(2,1)}, u32[]{:S(2)}) copy-start(bf16[2,256]{1,0:T(2,128)(2,1)} %get-tuple-element.16) | copy-start | bytes 3076
  108.8 2.5 %copy-start = (bf16[16,128,128]{2,1,0:T(8,128)(2,1)S(1)}, bf16[16,128,128]{2,1,0:T(8,128)(2,1)}, u32[]{:S(2)}) copy-start(bf16[16,128,128]{2,1,0:T(8,128)(2,1)} %get-tuple-element.8) | copy-start | bytes 1572868

commit v2 on v1

--- a/solution.py
+++ b/solution.py
@@ -330,21 +330,6 @@
     return one(ah, bh) + (one(ah, bl) + one(al, bh))
 
 
-def choose(table, index):
-    value = jnp.int32(table[0])
-    for at in range(1, len(table)):
-        value = jnp.where(index == at, jnp.int32(table[at]), value)
-    return value
-
-
-def by_distance(k):
-    order = []
-    for z in range(DEEP):
-        others = sorted((abs(o - z), o) for o in range(DEEP) if o != z)
-        order.append(others[k - 1][1])
-    return order
-
-
 def prefill_kernel(
     peers,
     tok,
@@ -373,6 +358,7 @@
     addv,
     logit,
     msg,
+    gz,
     gall,
     keep,
     give,
@@ -397,8 +383,9 @@
     c_recv,
     relay_send,
     cross_send,
-    outer_send,
     blk_recv,
+    gz_send,
+    gz_recv,
     g_send,
     g_recv,
     give_send,
@@ -448,6 +435,14 @@
         ref = xall.at[c, part_of(i)]
         remote(ref, ref, own_sem, tok_recv.at[c, i], s, t).wait_recv()
 
+    near = [z, mate, DEEP - 1 - z, (z + DEEP // 2) % DEEP]
+    barrier = pltpu.get_barrier_semaphore()
+    partners = [(chip(x, y, near[k]), t) for k in range(1, DEEP)] + [(s, 1 - t)]
+    partners += [(c, core) for c in (x_peer, y_peer, diagonal) for core in (t, 1 - t)]
+    for c, core in partners:
+        pl.semaphore_signal(
+            barrier, inc=1, device_id={"sp": c, "tp": core}, device_id_type=MESH
+        )
     loads = []
     for i, (src, dst) in enumerate(
         (
@@ -461,13 +456,15 @@
         copy = pltpu.make_async_copy(src, dst, load.at[i])
         copy.start()
         loads.append(copy)
-
-    near = [z] + [choose(by_distance(k), z) for k in range(1, DEEP)]
-    for k in range(1, DEEP):
+    own = pltpu.make_async_copy(tok.at[prompt, :, columns], xall.at[s], own_sem)
+    own.start()
+    pl.semaphore_wait(barrier, len(partners))
+
+    def along_z(k, source):
         for i in range(PIECES):
             go(
                 remote(
-                    tok.at[near[k] % 2, part_of(i), columns],
+                    source.at[near[k] % 2, part_of(i), columns],
                     xall.at[s, part_of(i)],
                     z_send.at[k, i],
                     tok_recv.at[s, i],
@@ -475,8 +472,9 @@
                     t,
                 )
             )
-    own = pltpu.make_async_copy(tok.at[prompt, :, columns], xall.at[s], own_sem)
-    own.start()
+
+    along_z(1, tok)
+    along_z(2, tok)
 
     side_of = (t + side) % 2
     own_row = s % (peers // 2)
@@ -517,81 +515,71 @@
         go(remote(src, dst, x_send.at[0, i], tok_recv.at[s, i], x_peer, t))
         go(remote(src, dst, y_send.at[0, i], tok_recv.at[s, i], y_peer, t))
 
-    loads[0].wait()
-    loads[1].wait()
-    loads[2].wait()
-    loads[3].wait()
-    total_heads = gate_b.shape[0]
-    msg[...] = jnp.zeros_like(msg)
-    for p in range(2):
-        for kind in range(2):
-            logit[p, kind] = (
-                lax.dot_general(gatev[kind], tokv[p], NT, preferred_element_type=jnp.float32)
-                .astype(jnp.bfloat16)
-                .astype(jnp.float32)
-            )
-        for h in range(heads):
+    def gates():
+        for copy in loads[:4]:
+            copy.wait()
+        msg[...] = jnp.zeros_like(msg)
+        for p in range(2):
             for kind in range(2):
-                msg[p, h, kind : kind + 1, :] = logit[p, kind, pl.ds(t * heads + h, 1), :]
-            msg[p, h, 2:3, :] = addv[p, h : h + 1, :]
-    for off in range(1, peers):
-        to = (s + off) % peers
-        to_z = to // PLANE
-        go(
-            remote(
-                msg.at[to_z % 2, (to_z // 2) * PLANE + to % PLANE],
-                gall.at[s],
-                g_send.at[off],
-                g_recv.at[s],
-                to,
-                t,
-            )
-        )
-    gall[s] = msg[prompt, j]
-
-    def home_relay(dx, dy):
-        q = 2 * ((y + dy) % 2) + (x + dx) % 2
-        row = prompt * PLANE + q
-        block = wall.at[pl.ds(pl.multiple_of(row * rows, 16), rows)]
-        landing = chip(x, y, DEEP // 2 - side)
+                logit[p, kind] = (
+                    lax.dot_general(gatev[kind], tokv[p], NT, preferred_element_type=jnp.float32)
+                    .astype(jnp.bfloat16)
+                    .astype(jnp.float32)
+                )
+            for h in range(heads):
+                for kind in range(2):
+                    msg[p, h, kind : kind + 1, :] = logit[p, kind, pl.ds(t * heads + h, 1), :]
+                msg[p, h, 2:3, :] = addv[p, h : h + 1, :]
+        for k in range(1, DEEP):
+            src = msg.at[near[k] % 2, pl.ds(near[k] // 2 * PLANE, PLANE)]
+            go(remote(src, gz.at[z], gz_send.at[k], gz_recv.at[z], chip(x, y, near[k]), t))
+        for n, c in enumerate((x_peer, y_peer, diagonal)):
+            src = msg.at[prompt, side * PLANE + c % PLANE]
+            go(remote(src, gall.at[s], g_send.at[0, n], g_recv.at[s], c, t))
+        gall[s] = msg[prompt, j]
+
+    def pass_gates(k):
+        cz = near[k]
+        remote(gz.at[cz], gz.at[cz], own_sem, gz_recv.at[cz], s, t).wait_recv()
+        c = chip(x, y, cz)
+        for n, to in enumerate((x_peer, y_peer, diagonal)):
+            go(remote(gz.at[cz, to % PLANE], gall.at[c], g_send.at[k, n], g_recv.at[c], to, t))
+        gall[c] = gz[cz, q_own]
+
+    def block_of(row):
+        return wall.at[pl.ds(pl.multiple_of(row * rows, 16), rows)]
+
+    def row_at(n):
+        q = 2 * ((y + n // 2) % 2) + (x + n % 2) % 2
+        return q, prompt * PLANE + q
+
+    def home_relay(n):
+        q, row = row_at(n)
+        block = block_of(row)
+        landing = chip(x, y, (z + DEEP // 2) % DEEP)
         for c in range(4):
             one = wcross.at[q, :, pl.ds(c * width, width)]
             pltpu.make_async_copy(one, one, c_recv.at[q, c]).wait()
-        remote(
-            wcross.at[q], block, cross_send.at[q], blk_recv.at[row], landing, t
-        ).start()
+        remote(wcross.at[q], block, cross_send.at[q], blk_recv.at[row], landing, t).start()
         for c in range(4):
-            one = wall.at[
-                pl.ds(pl.multiple_of(row * rows, 16), rows), pl.ds(c * width, width)
-            ]
+            one = block.at[:, pl.ds(c * width, width)]
             pltpu.make_async_copy(one, one, w_recv.at[row, c]).wait()
         remote(block, block, relay_send.at[q], blk_recv.at[row], z_peer, t).start()
 
-    inner = prompt != side
-    lands = jnp.logical_and(jnp.logical_not(home), inner)
-
-    def block_of(row):
-        return wall.at[pl.ds(pl.multiple_of(row * rows, 16), rows)]
-
     def land_relay(n):
-        row = arrival_row(n)
+        q, row = row_at(n)
         ref = block_of(row)
-        remote(ref, ref, outer_send.at[n], blk_recv.at[row], s, t).wait_recv()
-        remote(ref, ref, outer_send.at[n], blk_recv.at[row], z_peer, t).start()
-
-    def arrival_row(n):
-        plane = (side + n) % 2
-        step = n // 2
-        q = 2 * ((y + step // 2) % 2) + (x + step % 2) % 2
-        return plane * PLANE + q
-
-    def on_home(dx, dy):
+        remote(ref, ref, relay_send.at[q], blk_recv.at[row], s, t).wait_recv()
+        remote(ref, ref, relay_send.at[q], blk_recv.at[row], z_peer, t).start()
+
+    def on_home(*ns):
         @pl.when(home)
         def _():
-            home_relay(dx, dy)
-
-    def on_land(ns):
-        @pl.when(lands)
+            for n in ns:
+                home_relay(n)
+
+    def on_land(*ns):
+        @pl.when(jnp.logical_not(home))
         def _():
             for n in ns:
                 land_relay(n)
@@ -614,45 +602,45 @@
         ref = xall.at[c, part_of(1)]
         go(remote(ref, ref, xf_send.at[k], tok_recv.at[c, 1], x_peer, t))
 
-    on_home(0, 0)
-    on_home(1, 0)
-    on_home(0, 1)
+    on_home(0)
+    gates()
+    on_home(1, 2)
+    on_land(0)
     spread_column(1)
-    on_home(1, 1)
+    along_z(3, tokv)
+    on_home(3)
+    on_land(1)
     cross_plane(0)
-    on_land((0, 1))
+    pass_gates(1)
+    on_land(2)
     spread_column(2)
+    on_land(3)
     cross_plane(1)
-    on_land((2, 3))
+    pass_gates(2)
     spread_column(3)
-    on_land((4, 5))
+    pass_gates(3)
     cross_plane(2)
-    on_land((6, 7))
     cross_plane(3)
 
     for n in range(PLANE):
-
-        @pl.when(home)
-        def _():
-            row = (1 - prompt) * PLANE + n
-            ref = block_of(row)
-            remote(ref, ref, own_sem, blk_recv.at[row], s, t).wait_recv()
-
-    for row in range(2 * PLANE):
-
-        @pl.when(jnp.logical_and(jnp.logical_not(home), jnp.logical_not(inner)))
-        def _():
-            ref = block_of(row)
-            remote(ref, ref, own_sem, blk_recv.at[row], s, t).wait_recv()
+        row = (1 - prompt) * PLANE + n
+        ref = block_of(row)
+        remote(ref, ref, own_sem, blk_recv.at[row], s, t).wait_recv()
 
     own.wait()
-    for off in range(1, peers):
-        c = (s + off) % peers
-        remote(gall.at[c], gall.at[c], own_sem, g_recv.at[c], s, t).wait_recv()
+    for off in range(1, PLANE):
+        for cz in near:
+            c = PLANE * cz + (s + off) % PLANE
+            remote(gall.at[c], gall.at[c], own_sem, g_recv.at[c], s, t).wait_recv()
+
+    def plane_of(g):
+        value = near[0]
+        for k in range(1, DEEP):
+            value = jnp.where(g == k, near[k], value)
+        return value
 
     def slots_of(g):
-        cx, cy = (x + g % 2) % 2, (y + g // 2) % 2
-        return [chip(cx, cy, k) for k in range(DEEP)]
+        return [PLANE * plane_of(g) + q for q in range(PLANE)]
 
     def exchange(c):
         return remote(give.at[c], got.at[c], give_send.at[c], give_recv.at[c], s, 1 - t)
@@ -660,16 +648,11 @@
     def project(g):
         slots = slots_of(g)
 
-        @pl.when(g % 2 == 1)
-        def _():
-            for c in slots:
-                token_wait(c, 1)
-
-        @pl.when(g // 2 == 1)
-        def _():
-            for c in slots:
-                token_wait(c, 0)
-
+        cz = plane_of(g)
+        token_wait(chip(1 - x, y, cz), 1)
+        token_wait(chip(x, 1 - y, cz), 0)
+        token_wait(chip(1 - x, 1 - y, cz), 0)
+        token_wait(chip(1 - x, 1 - y, cz), 1)
         rows_in = jnp.concatenate([xall[c] for c in slots], axis=0)
         wide = jnp.dot(rows_in, wall[...], preferred_element_type=jnp.float32)
         for i, c in enumerate(slots):
@@ -679,23 +662,28 @@
         for c in slots:
             exchange(c).start()
 
-    many = DEEP * length
-
-    def local(g):
-        slots = slots_of(g)
-        for c in slots:
-            exchange(c).wait_recv()
-        wide = jnp.concatenate([keep[c] + got[c] for c in slots], axis=0)
+    many = PLANE * length
+
+    def left_form(full):
+        two = full[:, : many // 2] + full[:, many // 2 :]
+        high, low = halves(two + pltpu.roll(two, length, 1))
+        return jnp.concatenate([high, low], axis=1)
+
+    def right_form(full):
+        blocks = [full[i * length : (i + 1) * length] for i in range(PLANE)]
+        high, low = halves((blocks[0] + blocks[1]) + (blocks[2] + blocks[3]))
+        return jnp.concatenate([high, low, high, low], axis=0)
+
+    def one_dot(a, b, dims=NN):
+        return lax.dot_general(a, b, dims, preferred_element_type=jnp.float32)
+
+    def maps_of(wide, bare_beta, bare_decay, added_decay):
         acted = silu(wide.astype(jnp.bfloat16).astype(jnp.float32))
         k = acted[:, :width]
         k = k * lax.rsqrt(jnp.sum(k * k, axis=-1, keepdims=True) + EPSILON)
         v = acted[:, width:]
-
-        def row_of(kind):
-            return jnp.concatenate([gall[c, kind : kind + 1, :] for c in slots], axis=1)
-
-        beta_row = sigmoid(row_of(0) + offset[j])
-        fade_row = row_of(2) - speed[j] * softplus(row_of(1))
+        beta_row = sigmoid(bare_beta + offset[j])
+        fade_row = added_decay - speed[j] * softplus(bare_decay)
         r = lax.broadcasted_iota(jnp.int32, (many, many), 0)
         c = lax.broadcasted_iota(jnp.int32, (many, many), 1)
         same = r // length == c // length
@@ -704,6 +692,9 @@
 
         def column(mask, row):
             return jnp.sum(jnp.where(mask, row, 0.0), axis=1, keepdims=True)
+
+        def kept(full):
+            return jnp.where(same, full, 0.0)
 
         sum_col = column(jnp.logical_and(same, r >= c), fade_row)
         all_col = column(same, fade_row)
@@ -712,44 +703,59 @@
         scaled = k * beta_col
         inner_products = dot3(halves(scaled), halves(k), NT)
         spread = jnp.exp(jnp.where(strict, sum_col - sum_row, 0.0))
-        power = halves(jnp.where(strict, inner_products * spread, 0.0))
-        solved = jnp.concatenate([scaled * jnp.exp(sum_col), v * beta_col], axis=1)
-        solved = solved - dot3(power, halves(solved))
+        lower = jnp.where(strict, inner_products * spread, 0.0)
+        left, right = left_form(lower), right_form(lower)
+        inverse = jnp.where(eye, 1.0, 0.0) - lower
         reached = 2
         while reached < length:
-            power = halves(dot3(power, power))
-            solved = solved + dot3(power, halves(solved))
+            power = kept(one_dot(left, right))
+            right = right_form(power)
+            inverse = inverse + kept(one_dot(left_form(inverse), right))
             reached *= 2
+            if reached < length:
+                left = left_form(power)
+        inverse = left_form(inverse)
+        targets = halves(jnp.concatenate([scaled * jnp.exp(sum_col), v * beta_col], axis=1))
         tail = halves(k * jnp.exp(all_col - sum_col))
-        solved = halves(solved)
+        last = jnp.exp(all_col)
         unit = (
             lax.broadcasted_iota(jnp.int32, (width, width), 0)
             == lax.broadcasted_iota(jnp.int32, (width, width), 1)
         ).astype(jnp.float32)
-        last = jnp.exp(all_col)
-        for i, slot in enumerate(slots):
+        pairs = []
+        for i in range(PLANE):
             at = slice(i * length, (i + 1) * length)
-            maps = dot3(
-                tuple(a[at] for a in tail), tuple(a[at] for a in solved), TN
-            )
+            high, low = targets[0][at], targets[1][at]
+            solved = one_dot(inverse[at], jnp.concatenate([high, low, high, low], axis=0))
+            high, low = halves(solved)
+            keys = jnp.concatenate([tail[0][at]] * 2 + [tail[1][at]] * 2, axis=0)
+            maps = one_dot(keys, jnp.concatenate([high, low, high, low], axis=0), TN)
             moves = last[i * length : i * length + 1] * unit - maps[:, :width]
-            pair[slot, :, :width] = moves
-            pair[slot, :, width:] = maps[:, width:]
-
-    groups = peers // DEEP
-
-    def stage(g, carry):
-        @pl.when(g < groups)
-        def _():
-            project(g)
-
-        @pl.when(g > 0)
-        def _():
-            local(g - 1)
-
-        return carry
-
-    lax.fori_loop(0, groups + 1, stage, 0)
+            pairs.append((moves, maps[:, width:]))
+        return pairs
+
+    def local(n):
+        slots = [slots_of(2 * n + i) for i in range(2)]
+        for group in slots:
+            for c in group:
+                exchange(c).wait_recv()
+        given = []
+        for group in slots:
+
+            def row_of(kind, group=group):
+                return jnp.concatenate([gall[c, kind : kind + 1, :] for c in group], axis=1)
+
+            wide = jnp.concatenate([keep[c] + got[c] for c in group], axis=0)
+            given.append((wide, row_of(0), row_of(1), row_of(2)))
+        found = [maps_of(*g) for g in given]
+        for group, pairs in zip(slots, found):
+            for slot, (moves, shift) in zip(group, pairs):
+                pair[slot, :, :width] = moves
+                pair[slot, :, width:] = shift
+
+    groups = peers // PLANE
+    lax.fori_loop(0, groups, lambda g, carry: (project(g), carry)[1], 0)
+    lax.fori_loop(0, groups // 2, lambda n, carry: (local(n), carry)[1], 0)
 
     chains = []
     for g in range(groups):
@@ -816,7 +822,7 @@
         go(remote(rmsg, rall.at[slot], r_send.at[off], r_recv.at[slot], to, t))
     rall[slot] = rmsg[...]
 
-    others = [near[k] for k in range(1, DEEP)]
+    others = near[1:]
     for cz in others:
         pass_on(slot, chip(x, y, cz))
     pass_on(slot, y_peer)
@@ -865,19 +871,14 @@
     for copy in sent:
         copy.wait_send()
 
-    @pl.when(home)
-    def _():
-        for q in range(PLANE):
-            row = prompt * PLANE + q
-            ref = block_of(row)
+    for q in range(PLANE):
+        row = prompt * PLANE + q
+        ref = block_of(row)
+        remote(ref, ref, relay_send.at[q], blk_recv.at[row], s, t).wait_send()
+
+        @pl.when(home)
+        def _():
             remote(wcross.at[q], ref, cross_send.at[q], blk_recv.at[row], s, t).wait_send()
-            remote(ref, ref, relay_send.at[q], blk_recv.at[row], s, t).wait_send()
-
-    @pl.when(lands)
-    def _():
-        for n in range(2 * PLANE):
-            ref = block_of(arrival_row(n))
-            remote(ref, ref, outer_send.at[n], own_sem, s, t).wait_send()
 
     @pl.when(jnp.logical_not(home))
     def _():
@@ -921,6 +922,7 @@
             pltpu.VMEM(add.shape, f32),
             pltpu.VMEM((2, 2, gate_b.shape[0], length), f32),
             pltpu.VMEM((2, heads, 8, length), f32),
+            pltpu.VMEM((DEEP, PLANE, 8, length), f32),
             pltpu.VMEM((peers, 8, length), f32),
             pltpu.VMEM((peers, length, 2 * width), f32),
             pltpu.VMEM((peers, length, 2 * width), f32),
@@ -946,8 +948,9 @@
             dma((PLANE,)),
             dma((PLANE,)),
             dma((2 * PLANE,)),
-            dma((2 * PLANE,)),
-            dma((peers,)),
+            dma((DEEP,)),
+            dma((DEEP,)),
+            dma((DEEP, PLANE)),
             dma((peers,)),
             dma((peers,)),
             dma((peers,)),
@@ -960,7 +963,7 @@
             dma(()),
             dma(()),
         ],
-        compiler_params=pltpu.CompilerParams(has_side_effects=True),
+        compiler_params=pltpu.CompilerParams(has_side_effects=True, collective_id=0),
         name="prefill",
     )(tok, wk, wv, gate_b, gate_a, add, offset, speed, *first, strength, gain, readout)
 

time: 112 us -> 103 us (0.920)
  Pallas kernels: 108 us -> 99 us
    pallas_call x1, Pallas kernels: 108 us -> 99 us  [prefill(): pl.pallas_call(lambda *refs: prefill_kernel(peers, *refs), out_shape=(jax...]
where the time goes in v2:
time: 103 us
  Pallas kernels  99 us (96%)
  local copies, waits for them, and re-layouts  3.31 us (3%)
    pallas_call x1, Pallas kernels, prefill(): pl.pallas_call(lambda *refs: prefill_kernel(peers, *refs), out_shape=(jax...  99 us
    unnamed x7, local copies, waits for them, and re-layouts  3.31 us

profile of v2, /device:TPU:0, one launch (start us, length us, event | category | flops | bytes accessed | tf_op | source)
XLA Modules:
  0.0 102.9 jit_solution(12506826629830991861)
XLA Ops:
  0.6 99.0 %prefill.1 = (bf16[16,128,128]{2,1,0:T(8,128)(2,1)}, bf16[16,128,128]{2,1,0:T(8,128)(2,1)}, bf16[2,256]{1,0:T(2,128)(2,1)}) custom-call(bf16[2,64,4096]{2,1,0:T(8,128)(2,1)} %refs_0_.1, bf16[256,1024]{1,0:T(8,128)(2,1)} %refs_1_.1, bf16[256,1024]{1,0:T(8,128)(2,1)} %refs_2_.1, bf16[16,4096]{1,0:T(8,128)(2,1)} %bitcast.10, bf16[16,4096]{1,0:T(8,128)(2,1)} %bitcast.11, ...), custom_call_target="tpu_custom_call" | custom-call | tf_op jit(solution)/shard_map/prefill/pallas_call | solution.py:907
  99.6 0.0 copy-start.1
  99.6 0.0 copy-start
  99.6 1.9 %copy.22 = bf16[2,8,128,128]{3,2,1,0:T(8,128)(2,1)} copy(bf16[2,8,128,128]{3,2,1,0:T(8,128)(2,1)} %bitcast.9) | data formatting | bytes 1048576
  101.6 0.0 copy-done.1
  101.6 0.6 copy.23
  102.1 0.0 copy-done
  102.1 0.8 copy.24
Async XLA Ops:
  99.6 2.0 %copy-start.1 = (bf16[2,256]{1,0:T(2,128)(2,1)S(1)}, bf16[2,256]{1,0:T(2,128)(2,1)}, u32[]{:S(2)}) copy-start(bf16[2,256]{1,0:T(2,128)(2,1)} %get-tuple-element.16) | copy-start | bytes 3076
  99.6 2.5 %copy-start = (bf16[16,128,128]{2,1,0:T(8,128)(2,1)S(1)}, bf16[16,128,128]{2,1,0:T(8,128)(2,1)}, u32[]{:S(2)}) copy-start(bf16[16,128,128]{2,1,0:T(8,128)(2,1)} %get-tuple-element.8) | copy-start | bytes 1572868

commit v3 on v2

--- a/solution.py
+++ b/solution.py
@@ -322,14 +322,6 @@
 TN = (((0,), (0,)), ((), ()))
 
 
-def dot3(a, b, dims=NN):
-    def one(p, q):
-        return lax.dot_general(p, q, dims, preferred_element_type=jnp.float32)
-
-    (ah, al), (bh, bl) = a, b
-    return one(ah, bh) + (one(ah, bl) + one(al, bh))
-
-
 def prefill_kernel(
     peers,
     tok,
@@ -347,9 +339,11 @@
     strength,
     gain,
     readout,
+    final_out,
+    bound_out,
+    mixed,
     final,
     bound,
-    mixed,
     xall,
     wall,
     wcross,
@@ -363,7 +357,6 @@
     keep,
     give,
     got,
-    pair,
     states,
     rv,
     rmsg,
@@ -398,6 +391,8 @@
     r_recv,
     t_send,
     t_recv,
+    final_sem,
+    bound_sem,
 ):
     s, t = lax.axis_index("sp"), lax.axis_index("tp")
     heads = add.shape[1]
@@ -602,6 +597,37 @@
         ref = xall.at[c, part_of(1)]
         go(remote(ref, ref, xf_send.at[k], tok_recv.at[c, 1], x_peer, t))
 
+    def plane_of(g):
+        value = near[0]
+        for k in range(1, DEEP):
+            value = jnp.where(g == k, near[k], value)
+        return value
+
+    def slots_of(g):
+        return [PLANE * plane_of(g) + q for q in range(PLANE)]
+
+    def exchange(c):
+        return remote(give.at[c], got.at[c], give_send.at[c], give_recv.at[c], s, 1 - t)
+
+    deep_rows = PLANE * rows
+
+    def project(g, parity, first):
+        slots = slots_of(g)
+        depth = pl.ds(pl.multiple_of(parity * deep_rows, 128), deep_rows)
+        rows_in = jnp.concatenate([xall[c, :, depth] for c in slots], axis=0)
+        wide = jnp.dot(rows_in, wall[depth], preferred_element_type=jnp.float32)
+        for i, c in enumerate(slots):
+            part_rows = slice(i * length, (i + 1) * length)
+            mine, theirs = wide[part_rows, : 2 * width], wide[part_rows, 2 * width :]
+            if first:
+                keep[c], give[c] = mine, theirs
+            else:
+                keep[c] += mine
+                give[c] += theirs
+        if not first:
+            for c in slots:
+                exchange(c).start()
+
     on_home(0)
     gates()
     on_home(1, 2)
@@ -622,45 +648,27 @@
     cross_plane(2)
     cross_plane(3)
 
-    for n in range(PLANE):
-        row = (1 - prompt) * PLANE + n
-        ref = block_of(row)
-        remote(ref, ref, own_sem, blk_recv.at[row], s, t).wait_recv()
-
-    own.wait()
-    for off in range(1, PLANE):
-        for cz in near:
-            c = PLANE * cz + (s + off) % PLANE
-            remote(gall.at[c], gall.at[c], own_sem, g_recv.at[c], s, t).wait_recv()
-
-    def plane_of(g):
-        value = near[0]
-        for k in range(1, DEEP):
-            value = jnp.where(g == k, near[k], value)
-        return value
-
-    def slots_of(g):
-        return [PLANE * plane_of(g) + q for q in range(PLANE)]
-
-    def exchange(c):
-        return remote(give.at[c], got.at[c], give_send.at[c], give_recv.at[c], s, 1 - t)
-
-    def project(g):
-        slots = slots_of(g)
-
+    def token_rest(g, carry):
         cz = plane_of(g)
         token_wait(chip(1 - x, y, cz), 1)
         token_wait(chip(x, 1 - y, cz), 0)
         token_wait(chip(1 - x, 1 - y, cz), 0)
         token_wait(chip(1 - x, 1 - y, cz), 1)
-        rows_in = jnp.concatenate([xall[c] for c in slots], axis=0)
-        wide = jnp.dot(rows_in, wall[...], preferred_element_type=jnp.float32)
-        for i, c in enumerate(slots):
-            part_rows = slice(i * length, (i + 1) * length)
-            keep[c] = wide[part_rows, : 2 * width]
-            give[c] = wide[part_rows, 2 * width :]
-        for c in slots:
-            exchange(c).start()
+        project(g, prompt, True)
+        return carry
+
+    own.wait()
+    lax.fori_loop(0, DEEP, token_rest, 0)
+
+    for n in range(PLANE):
+        row = (1 - prompt) * PLANE + n
+        ref = block_of(row)
+        remote(ref, ref, own_sem, blk_recv.at[row], s, t).wait_recv()
+
+    for off in range(1, PLANE):
+        for cz in near:
+            c = PLANE * cz + (s + off) % PLANE
+            remote(gall.at[c], gall.at[c], own_sem, g_recv.at[c], s, t).wait_recv()
 
     many = PLANE * length
 
@@ -676,6 +684,10 @@
 
     def one_dot(a, b, dims=NN):
         return lax.dot_general(a, b, dims, preferred_element_type=jnp.float32)
+
+    def packed_dot(a, b):
+        first = one_dot(jnp.concatenate(a, axis=1), jnp.concatenate([b[0], b[0]], axis=0))
+        return first + one_dot(a[0], b[1])
 
     def maps_of(wide, bare_beta, bare_decay, added_decay):
         acted = silu(wide.astype(jnp.bfloat16).astype(jnp.float32))
@@ -701,7 +713,10 @@
         beta_col = column(eye, beta_row)
         sum_row = jnp.sum(jnp.where(eye, sum_col, 0.0), axis=0, keepdims=True)
         scaled = k * beta_col
-        inner_products = dot3(halves(scaled), halves(k), NT)
+        (high, low), (k_high, k_low) = halves(scaled), halves(k)
+        inner_products = one_dot(
+            jnp.concatenate([high, low], axis=1), jnp.concatenate([k_high, k_high], axis=1), NT
+        ) + one_dot(high, k_low, NT)
         spread = jnp.exp(jnp.where(strict, sum_col - sum_row, 0.0))
         lower = jnp.where(strict, inner_products * spread, 0.0)
         left, right = left_form(lower), right_form(lower)
@@ -734,55 +749,47 @@
             pairs.append((moves, maps[:, width:]))
         return pairs
 
-    def local(n):
-        slots = [slots_of(2 * n + i) for i in range(2)]
-        for group in slots:
-            for c in group:
-                exchange(c).wait_recv()
-        given = []
-        for group in slots:
-
-            def row_of(kind, group=group):
-                return jnp.concatenate([gall[c, kind : kind + 1, :] for c in group], axis=1)
-
-            wide = jnp.concatenate([keep[c] + got[c] for c in group], axis=0)
-            given.append((wide, row_of(0), row_of(1), row_of(2)))
-        found = [maps_of(*g) for g in given]
-        for group, pairs in zip(slots, found):
-            for slot, (moves, shift) in zip(group, pairs):
-                pair[slot, :, :width] = moves
-                pair[slot, :, width:] = shift
+    def join(late, early):
+        both = packed_dot(halves(late[0]), halves(jnp.concatenate(early, axis=1)))
+        return both[:, :width], both[:, width:] + late[1]
 
     groups = peers // PLANE
-    lax.fori_loop(0, groups, lambda g, carry: (project(g), carry)[1], 0)
-    lax.fori_loop(0, groups // 2, lambda n, carry: (local(n), carry)[1], 0)
-
-    chains = []
+    lax.fori_loop(0, groups, lambda g, carry: (project(g, 1 - prompt, False), carry)[1], 0)
+
+    for c in range(peers):
+        exchange(c).wait_recv()
+    slot = slot_of(s)
+    carried = None
     for g in range(groups):
-        first = pair[g * DEEP]
-        chain = [(first[:, :width], first[:, width:])]
-        for i in range(1, DEEP):
-            late = pair[g * DEEP + i]
-            before = jnp.concatenate(chain[-1], axis=1)
-            joined = dot3(halves(late[:, :width]), halves(before))
-            chain.append((joined[:, :width], joined[:, width:] + late[:, width:]))
-        chains.append(chain)
-    carry = None
-    found = {}
-    for g in range(groups):
-        move, shift = chains[g][-1]
-        if carry is not None:
-            move = halves(move)
-            shift = dot3(move, carry[0]) + shift
-        found[g * DEEP + DEEP - 1] = shift
-        for i in range(DEEP - 1):
-            found_shift = chains[g][i][1]
-            if carry is not None:
-                found_shift = dot3(halves(chains[g][i][0]), carry[0]) + found_shift
-            found[g * DEEP + i] = found_shift
-        carry = (halves(shift),)
-    slot = slot_of(s)
-    end = found[peers - 1].astype(jnp.bfloat16)
+        slots = range(g * PLANE, (g + 1) * PLANE)
+
+        def row_of(kind, slots=slots):
+            return jnp.concatenate([gall[c, kind : kind + 1, :] for c in slots], axis=1)
+
+        wide = jnp.concatenate([keep[c] + got[c] for c in slots], axis=0)
+        pairs = maps_of(wide, row_of(0), row_of(1), row_of(2))
+        second = join(pairs[1], pairs[0])
+        chain = [pairs[0], second, join(pairs[2], second), join(join(pairs[3], pairs[2]), second)]
+        shifts = [shift for _, shift in chain]
+        if carried is not None:
+            shifts = [
+                packed_dot(halves(move), carried) + shift for move, shift in chain
+            ]
+        carried = halves(shifts[-1])
+        for c, shift in zip(slots, shifts):
+            states[c] = shift.astype(jnp.bfloat16)
+        if g == groups - 1:
+            break
+        for off in (1, 2, 3, 0):
+            to = g * PLANE + (s + off) % PLANE
+            copy = remote(
+                states.at[to], bound.at[slot], b_send.at[g, off], b_recv.at[slot], to, t
+            )
+            if off:
+                go(copy)
+            else:
+                pl.when(z != g)(copy.start)
+    end = shifts[-1].astype(jnp.bfloat16)
     final[slot] = end
     f_sent = [0]
 
@@ -792,9 +799,20 @@
         ref = final.at[slot_at]
         go(remote(ref, ref, f_send.at[n], f_recv.at[slot_at], to, t))
 
+    def store_final(slot_at):
+        pltpu.make_async_copy(
+            final.at[slot_at], final_out.at[slot_at], final_sem.at[slot_at]
+        ).start()
+
+    def store_bound(slot_at):
+        pltpu.make_async_copy(
+            bound.at[slot_at], bound_out.at[slot_at], bound_sem.at[slot_at]
+        ).start()
+
     def arrived(slot_at):
         ref = final.at[slot_at]
         remote(ref, ref, own_sem, f_recv.at[slot_at], s, t).wait_recv()
+        store_final(slot_at)
 
     def own_row_of(ref):
         two = ref[:, pl.ds(pl.multiple_of(j * width, 128), width)].astype(jnp.float32)
@@ -827,22 +845,24 @@
         pass_on(slot, chip(x, y, cz))
     pass_on(slot, y_peer)
     pass_on(slot, x_peer)
-    for n in range(peers):
-        states[n] = found[n].astype(jnp.bfloat16)
-    for off in range(1, peers):
-        to = (s + off) % peers
-        go(remote(states.at[to], bound.at[slot], b_send.at[off], b_recv.at[slot], to, t))
+    last_plane = DEEP - 1
+    for off in (1, 2, 3, 0):
+        to = last_plane * PLANE + (s + off) % PLANE
+        copy = remote(
+            states.at[to], bound.at[slot], b_send.at[last_plane, off], b_recv.at[slot], to, t
+        )
+        if off:
+            go(copy)
+        else:
+            pl.when(z != last_plane)(copy.start)
     bound[slot] = states[s]
+    store_final(slot)
+    store_bound(slot)
     for cz in others:
         come = slot_of(chip(x, y, cz))
         arrived(come)
         pass_on(come, y_peer)
         pass_on(come, x_peer)
-    for cz in near:
-        come = slot_of(chip(x, 1 - y, cz))
-        arrived(come)
-        pass_on(come, x_peer)
-
     for off in range(1, peers):
         come = slot_of((s + off) % peers)
         remote(rall.at[come], rall.at[come], own_sem, r_recv.at[come], s, t).wait_recv()
@@ -860,6 +880,11 @@
     swap.wait()
     mixed[...] = (part[...] + partgot[...])[:2].astype(mixed.dtype)
 
+    for cz in near:
+        come = slot_of(chip(x, 1 - y, cz))
+        arrived(come)
+        pass_on(come, x_peer)
+
     for cz in range(DEEP):
         for cy in range(2):
             arrived(slot_of(chip(1 - x, cy, cz)))
@@ -867,7 +892,12 @@
         come = slot_of((s + off) % peers)
         ref = bound.at[come]
         remote(ref, ref, own_sem, b_recv.at[come], s, t).wait_recv()
-
+        store_bound(come)
+
+    for g in range(groups):
+        ref = states.at[g * PLANE + s % PLANE]
+        copy = remote(ref, bound.at[slot], b_send.at[g, 0], b_recv.at[slot], s, t)
+        pl.when(z != g)(copy.wait_send)
     for copy in sent:
         copy.wait_send()
 
@@ -891,6 +921,9 @@
         return carry
 
     lax.fori_loop(0, peers, give_done, 0)
+    for c in range(peers):
+        pltpu.make_async_copy(final.at[c], final_out.at[c], final_sem.at[c]).wait()
+        pltpu.make_async_copy(bound.at[c], bound_out.at[c], bound_sem.at[c]).wait()
 
 
 def prefill(tok, wk, wv, gate_b, gate_a, add, offset, speed, first, strength, gain, readout, peers):
@@ -912,8 +945,10 @@
             jax.ShapeDtypeStruct((2, readout.shape[1]), bf16),
         ),
         in_specs=[anywhere] * 6 + [smem] * 2 + [vmem] * 4 + [smem, vmem, anywhere],
-        out_specs=(vmem, vmem, vmem),
+        out_specs=(anywhere, anywhere, vmem),
         scratch_shapes=[
+            pltpu.VMEM((peers, width, width), bf16),
+            pltpu.VMEM((peers, width, width), bf16),
             pltpu.VMEM((peers, length, half), bf16),
             pltpu.VMEM((half, 4 * width), bf16),
             pltpu.VMEM((PLANE, rows, 4 * width), bf16),
@@ -927,7 +962,6 @@
             pltpu.VMEM((peers, length, 2 * width), f32),
             pltpu.VMEM((peers, length, 2 * width), f32),
             pltpu.VMEM((peers, length, 2 * width), f32),
-            pltpu.VMEM((peers, width, 2 * width), f32),
             pltpu.VMEM((peers, width, width), bf16),
             pltpu.VMEM(readout.shape, bf16),
             pltpu.VMEM((8, width), f32),
@@ -956,16 +990,51 @@
             dma((peers,)),
             dma((peers,)),
             dma((peers,)),
-            dma((peers,)),
+            dma((DEEP, PLANE)),
             dma((peers,)),
             dma((peers,)),
             dma((peers,)),
             dma(()),
             dma(()),
+            dma((peers,)),
+            dma((peers,)),
         ],
         compiler_params=pltpu.CompilerParams(has_side_effects=True, collective_id=0),
         name="prefill",
     )(tok, wk, wv, gate_b, gate_a, add, offset, speed, *first, strength, gain, readout)
+
+
+def hand_over(*arrays):
+    def kernel(*refs):
+        count = len(arrays)
+        sources, targets, held = (refs[i * count : (i + 1) * count] for i in range(3))
+        came, left = refs[3 * count :]
+        steps = []
+        for i in range(count):
+            steps.append(
+                (
+                    pltpu.make_async_copy(sources[i], held[i], came.at[i]),
+                    pltpu.make_async_copy(held[i], targets[i], left.at[i]),
+                )
+            )
+        for first, _ in steps:
+            first.start()
+        for first, second in steps:
+            first.wait()
+            second.start()
+        for _, second in steps:
+            second.wait()
+
+    anywhere = pl.BlockSpec(memory_space=pl.ANY)
+    return pl.pallas_call(
+        kernel,
+        out_shape=tuple(jax.ShapeDtypeStruct(a.shape, a.dtype) for a in arrays),
+        in_specs=[anywhere] * len(arrays),
+        out_specs=(anywhere,) * len(arrays),
+        scratch_shapes=[pltpu.VMEM(a.shape, a.dtype) for a in arrays]
+        + [pltpu.SemaphoreType.DMA((len(arrays),))] * 2,
+        name="hand_over",
+    )(*arrays)
 
 
 def per_device_heads(
@@ -1003,6 +1072,7 @@
         readout_projection,
         peers,
     )
+    final, bound, mixed = hand_over(final, bound, mixed)
     state_cache = final.reshape(2, head_local, width, width)
     boundary_cache = bound.reshape(2, 1, head_local, width, width)
     return (state_cache, mixed, boundary_cache)

time: 103 us -> 101 us (0.981); the launches traced: 103 us -> 99.9 us
  local copies, waits for them, and re-layouts: 3.31 us -> 0 us
    unnamed x7 -> x0, local copies, waits for them, and re-layouts: 3.31 us -> none
    pallas_call x0 -> x1, Pallas kernels: none -> 2.06 us  [hand_over(): pl.pallas_call(kernel, out_shape=tuple((jax.ShapeDtypeStruct(a.shape, a.d...]
    pallas_call x1, Pallas kernels: 99 us -> 97.2 us  [prefill(): pl.pallas_call(lambda *refs: prefill_kernel(peers, *refs), out_shape=(jax...]
where the time goes in v3:
time: 101 us; the launch traced here: 99.9 us
  Pallas kernels  99.2 us (98%)
    pallas_call x1, Pallas kernels, prefill(): pl.pallas_call(lambda *refs: prefill_kernel(peers, *refs), out_shape=(jax...  97.2 us
    pallas_call x1, Pallas kernels, hand_over(): pl.pallas_call(kernel, out_shape=tuple((jax.ShapeDtypeStruct(a.shape, a.d...  2.06 us

profile of v3, /device:TPU:0, one launch (start us, length us, event | category | flops | bytes accessed | tf_op | source)
XLA Modules:
  0.0 99.9 jit_solution(8182879371421740898)
XLA Ops:
  0.6 97.2 %prefill.1 = (bf16[16,128,128]{2,1,0:T(8,128)(2,1)}, bf16[16,128,128]{2,1,0:T(8,128)(2,1)}, bf16[2,256]{1,0:T(2,128)(2,1)}) custom-call(bf16[2,64,4096]{2,1,0:T(8,128)(2,1)} %refs_0_.1, bf16[256,1024]{1,0:T(8,128)(2,1)} %refs_1_.1, bf16[256,1024]{1,0:T(8,128)(2,1)} %refs_2_.1, bf16[16,4096]{1,0:T(8,128)(2,1)} %bitcast.8, bf16[16,4096]{1,0:T(8,128)(2,1)} %bitcast.9, ...), custom_call_target="tpu_custom_call" | custom-call | tf_op jit(solution)/shard_map/prefill/pallas_call | solution.py:940
  97.8 2.1 %hand_over.1 = (bf16[16,128,128]{2,1,0:T(8,128)(2,1)}, bf16[16,128,128]{2,1,0:T(8,128)(2,1)}, bf16[2,256]{1,0:T(2,128)(2,1)}) custom-call(bf16[16,128,128]{2,1,0:T(8,128)(2,1)} %get-tuple-element.9.refs_0_, bf16[16,128,128]{2,1,0:T(8,128)(2,1)} %get-tuple-element.10.refs_1_, bf16[2,256]{1,0:T(2,128)(2,1)} %get-tuple-element.11.refs_2_), custom_call_target="tpu_custom_call" | custom-call | tf_op jit(solution)/shard_map/hand_over/pallas_call | solution.py:1029

commit v4 on v3

--- a/solution.py
+++ b/solution.py
@@ -365,13 +365,10 @@
     partgot,
     load,
     own_sem,
-    z_send,
+    tok_send,
     tok_recv,
-    x_send,
-    y_send,
-    xf_send,
-    yf_send,
     w_send,
+    w_away,
     w_recv,
     c_recv,
     relay_send,
@@ -420,11 +417,12 @@
     def part_of(i):
         return pl.ds(i * piece, piece)
 
-    sent = []
-
-    def go(copy):
+    sent = {"tok": 0, "final": 0}
+
+    def go(copy, kind=None):
         copy.start()
-        sent.append(copy)
+        if kind:
+            sent[kind] += 1
 
     def token_wait(c, i):
         ref = xall.at[c, part_of(i)]
@@ -461,11 +459,12 @@
                 remote(
                     source.at[near[k] % 2, part_of(i), columns],
                     xall.at[s, part_of(i)],
-                    z_send.at[k, i],
+                    tok_send,
                     tok_recv.at[s, i],
                     chip(x, y, near[k]),
                     t,
-                )
+                ),
+                "tok",
             )
 
     along_z(1, tok)
@@ -482,10 +481,10 @@
         src = (wk, wv)[kv].at[:, pl.ds(pl.multiple_of(head * width, 128), width)]
         at = pl.ds(pl.multiple_of((2 * side_of + kv) * width, 128), width)
         if cross:
-            dst, sem = wcross.at[q_own, :, at], c_recv.at[q_own, 2 * side_of + kv]
+            dst, sem = wcross.at[q_own, :, at], c_recv.at[q_own]
         else:
-            dst, sem = wall.at[spot, at], w_recv.at[own_row, 2 * side_of + kv]
-        out = w_send.at[2 * dy + dx, 2 * cross + kv]
+            dst, sem = wall.at[spot, at], w_recv.at[q_own]
+        out = w_send if dx + dy else w_away
         return src, dst, sem, remote(src, dst, out, sem, chip(xd, yd, z), side)
 
     for dx, dy in ((0, 0), (1, 0), (0, 1), (1, 1)):
@@ -507,8 +506,8 @@
     for i in range(PIECES):
         src = tok.at[prompt, part_of(i), columns]
         dst = xall.at[s, part_of(i)]
-        go(remote(src, dst, x_send.at[0, i], tok_recv.at[s, i], x_peer, t))
-        go(remote(src, dst, y_send.at[0, i], tok_recv.at[s, i], y_peer, t))
+        go(remote(src, dst, tok_send, tok_recv.at[s, i], x_peer, t), "tok")
+        go(remote(src, dst, tok_send, tok_recv.at[s, i], y_peer, t), "tok")
 
     def gates():
         for copy in loads[:4]:
@@ -527,10 +526,10 @@
                 msg[p, h, 2:3, :] = addv[p, h : h + 1, :]
         for k in range(1, DEEP):
             src = msg.at[near[k] % 2, pl.ds(near[k] // 2 * PLANE, PLANE)]
-            go(remote(src, gz.at[z], gz_send.at[k], gz_recv.at[z], chip(x, y, near[k]), t))
+            go(remote(src, gz.at[z], gz_send, gz_recv.at[z], chip(x, y, near[k]), t))
         for n, c in enumerate((x_peer, y_peer, diagonal)):
             src = msg.at[prompt, side * PLANE + c % PLANE]
-            go(remote(src, gall.at[s], g_send.at[0, n], g_recv.at[s], c, t))
+            go(remote(src, gall.at[s], g_send, g_recv, c, t))
         gall[s] = msg[prompt, j]
 
     def pass_gates(k):
@@ -538,7 +537,7 @@
         remote(gz.at[cz], gz.at[cz], own_sem, gz_recv.at[cz], s, t).wait_recv()
         c = chip(x, y, cz)
         for n, to in enumerate((x_peer, y_peer, diagonal)):
-            go(remote(gz.at[cz, to % PLANE], gall.at[c], g_send.at[k, n], g_recv.at[c], to, t))
+            go(remote(gz.at[cz, to % PLANE], gall.at[c], g_send, g_recv, to, t))
         gall[c] = gz[cz, q_own]
 
     def block_of(row):
@@ -552,20 +551,16 @@
         q, row = row_at(n)
         block = block_of(row)
         landing = chip(x, y, (z + DEEP // 2) % DEEP)
-        for c in range(4):
-            one = wcross.at[q, :, pl.ds(c * width, width)]
-            pltpu.make_async_copy(one, one, c_recv.at[q, c]).wait()
-        remote(wcross.at[q], block, cross_send.at[q], blk_recv.at[row], landing, t).start()
-        for c in range(4):
-            one = block.at[:, pl.ds(c * width, width)]
-            pltpu.make_async_copy(one, one, w_recv.at[row, c]).wait()
-        remote(block, block, relay_send.at[q], blk_recv.at[row], z_peer, t).start()
+        pltpu.make_async_copy(wcross.at[q], wcross.at[q], c_recv.at[q]).wait()
+        remote(wcross.at[q], block, cross_send, blk_recv.at[row], landing, t).start()
+        pltpu.make_async_copy(block, block, w_recv.at[q]).wait()
+        remote(block, block, relay_send, blk_recv.at[row], z_peer, t).start()
 
     def land_relay(n):
         q, row = row_at(n)
         ref = block_of(row)
-        remote(ref, ref, relay_send.at[q], blk_recv.at[row], s, t).wait_recv()
-        remote(ref, ref, relay_send.at[q], blk_recv.at[row], z_peer, t).start()
+        remote(ref, ref, relay_send, blk_recv.at[row], s, t).wait_recv()
+        remote(ref, ref, relay_send, blk_recv.at[row], z_peer, t).start()
 
     def on_home(*ns):
         @pl.when(home)
@@ -584,18 +579,18 @@
             c = chip(x, y, near[k])
             token_wait(c, i)
             ref = xall.at[c, part_of(i)]
-            go(remote(ref, ref, x_send.at[k, i], tok_recv.at[c, i], x_peer, t))
-            go(remote(ref, ref, y_send.at[k, i], tok_recv.at[c, i], y_peer, t))
+            go(remote(ref, ref, tok_send, tok_recv.at[c, i], x_peer, t), "tok")
+            go(remote(ref, ref, tok_send, tok_recv.at[c, i], y_peer, t), "tok")
 
     def cross_plane(k):
         c = chip(1 - x, y, near[k])
         token_wait(c, 0)
         ref = xall.at[c, part_of(0)]
-        go(remote(ref, ref, yf_send.at[k], tok_recv.at[c, 0], y_peer, t))
+        go(remote(ref, ref, tok_send, tok_recv.at[c, 0], y_peer, t), "tok")
         c = chip(x, 1 - y, near[k])
         token_wait(c, 1)
         ref = xall.at[c, part_of(1)]
-        go(remote(ref, ref, xf_send.at[k], tok_recv.at[c, 1], x_peer, t))
+        go(remote(ref, ref, tok_send, tok_recv.at[c, 1], x_peer, t), "tok")
 
     def plane_of(g):
         value = near[0]
@@ -607,68 +602,49 @@
         return [PLANE * plane_of(g) + q for q in range(PLANE)]
 
     def exchange(c):
-        return remote(give.at[c], got.at[c], give_send.at[c], give_recv.at[c], s, 1 - t)
-
-    deep_rows = PLANE * rows
-
-    def project(g, parity, first):
+        return remote(give.at[c], got.at[c], give_send, give_recv, s, 1 - t)
+
+    def project(g):
         slots = slots_of(g)
-        depth = pl.ds(pl.multiple_of(parity * deep_rows, 128), deep_rows)
-        rows_in = jnp.concatenate([xall[c, :, depth] for c in slots], axis=0)
-        wide = jnp.dot(rows_in, wall[depth], preferred_element_type=jnp.float32)
-        for i, c in enumerate(slots):
-            part_rows = slice(i * length, (i + 1) * length)
-            mine, theirs = wide[part_rows, : 2 * width], wide[part_rows, 2 * width :]
-            if first:
-                keep[c], give[c] = mine, theirs
-            else:
-                keep[c] += mine
-                give[c] += theirs
-        if not first:
-            for c in slots:
-                exchange(c).start()
-
-    on_home(0)
-    gates()
-    on_home(1, 2)
-    on_land(0)
-    spread_column(1)
-    along_z(3, tokv)
-    on_home(3)
-    on_land(1)
-    cross_plane(0)
-    pass_gates(1)
-    on_land(2)
-    spread_column(2)
-    on_land(3)
-    cross_plane(1)
-    pass_gates(2)
-    spread_column(3)
-    pass_gates(3)
-    cross_plane(2)
-    cross_plane(3)
-
-    def token_rest(g, carry):
         cz = plane_of(g)
         token_wait(chip(1 - x, y, cz), 1)
         token_wait(chip(x, 1 - y, cz), 0)
         token_wait(chip(1 - x, 1 - y, cz), 0)
         token_wait(chip(1 - x, 1 - y, cz), 1)
-        project(g, prompt, True)
-        return carry
-
-    own.wait()
-    lax.fori_loop(0, DEEP, token_rest, 0)
+        rows_in = jnp.concatenate([xall[c] for c in slots], axis=0)
+        wide = jnp.dot(rows_in, wall[...], preferred_element_type=jnp.float32)
+        for i, c in enumerate(slots):
+            part_rows = slice(i * length, (i + 1) * length)
+            keep[c] = wide[part_rows, : 2 * width]
+            give[c] = wide[part_rows, 2 * width :]
+        for c in slots:
+            exchange(c).start()
+
+    on_home(0)
+    gates()
+    on_home(1, 2)
+    spread_column(1)
+    on_home(3)
+    cross_plane(0)
+    pass_gates(1)
+    on_land(0, 1)
+    along_z(3, tokv)
+    spread_column(2)
+    cross_plane(1)
+    pass_gates(2)
+    on_land(2, 3)
+    spread_column(3)
+    pass_gates(3)
+    cross_plane(2)
+    cross_plane(3)
 
     for n in range(PLANE):
         row = (1 - prompt) * PLANE + n
         ref = block_of(row)
         remote(ref, ref, own_sem, blk_recv.at[row], s, t).wait_recv()
 
-    for off in range(1, PLANE):
-        for cz in near:
-            c = PLANE * cz + (s + off) % PLANE
-            remote(gall.at[c], gall.at[c], own_sem, g_recv.at[c], s, t).wait_recv()
+    relayed = gall.at[pl.ds(0, DEEP * (PLANE - 1))]
+    pltpu.make_async_copy(relayed, relayed, g_recv).wait()
 
     many = PLANE * length
 
@@ -754,10 +730,10 @@
         return both[:, :width], both[:, width:] + late[1]
 
     groups = peers // PLANE
-    lax.fori_loop(0, groups, lambda g, carry: (project(g, 1 - prompt, False), carry)[1], 0)
-
-    for c in range(peers):
-        exchange(c).wait_recv()
+    own.wait()
+    lax.fori_loop(0, groups, lambda g, carry: (project(g), carry)[1], 0)
+
+    pltpu.make_async_copy(got, got, give_recv).wait()
     slot = slot_of(s)
     carried = None
     for g in range(groups):
@@ -783,7 +759,7 @@
         for off in (1, 2, 3, 0):
             to = g * PLANE + (s + off) % PLANE
             copy = remote(
-                states.at[to], bound.at[slot], b_send.at[g, off], b_recv.at[slot], to, t
+                states.at[to], bound.at[slot], b_send, b_recv, to, t
             )
             if off:
                 go(copy)
@@ -791,23 +767,12 @@
                 pl.when(z != g)(copy.start)
     end = shifts[-1].astype(jnp.bfloat16)
     final[slot] = end
-    f_sent = [0]
-
     def pass_on(slot_at, to):
-        n = f_sent[0]
-        f_sent[0] += 1
         ref = final.at[slot_at]
-        go(remote(ref, ref, f_send.at[n], f_recv.at[slot_at], to, t))
+        go(remote(ref, ref, f_send, f_recv.at[slot_at], to, t), "final")
 
     def store_final(slot_at):
-        pltpu.make_async_copy(
-            final.at[slot_at], final_out.at[slot_at], final_sem.at[slot_at]
-        ).start()
-
-    def store_bound(slot_at):
-        pltpu.make_async_copy(
-            bound.at[slot_at], bound_out.at[slot_at], bound_sem.at[slot_at]
-        ).start()
+        pltpu.make_async_copy(final.at[slot_at], final_out.at[slot_at], final_sem).start()
 
     def arrived(slot_at):
         ref = final.at[slot_at]
@@ -837,7 +802,7 @@
     rmsg[...] = jnp.broadcast_to(gated.astype(jnp.bfloat16).astype(jnp.float32), rmsg.shape)
     for off in range(1, peers):
         to = (s + off) % peers
-        go(remote(rmsg, rall.at[slot], r_send.at[off], r_recv.at[slot], to, t))
+        go(remote(rmsg, rall.at[slot], r_send, r_recv, to, t))
     rall[slot] = rmsg[...]
 
     others = near[1:]
@@ -849,7 +814,7 @@
     for off in (1, 2, 3, 0):
         to = last_plane * PLANE + (s + off) % PLANE
         copy = remote(
-            states.at[to], bound.at[slot], b_send.at[last_plane, off], b_recv.at[slot], to, t
+            states.at[to], bound.at[slot], b_send, b_recv, to, t
         )
         if off:
             go(copy)
@@ -857,15 +822,13 @@
             pl.when(z != last_plane)(copy.start)
     bound[slot] = states[s]
     store_final(slot)
-    store_bound(slot)
     for cz in others:
         come = slot_of(chip(x, y, cz))
         arrived(come)
         pass_on(come, y_peer)
         pass_on(come, x_peer)
-    for off in range(1, peers):
-        come = slot_of((s + off) % peers)
-        remote(rall.at[come], rall.at[come], own_sem, r_recv.at[come], s, t).wait_recv()
+    far = pl.ds(0, peers - 1)
+    pltpu.make_async_copy(rall.at[far], rall.at[far], r_recv).wait()
     lines = [
         jnp.concatenate([rall[p * heads + h, 0:1, :] for h in range(heads)], axis=1)
         for p in range(2)
@@ -888,42 +851,33 @@
     for cz in range(DEEP):
         for cy in range(2):
             arrived(slot_of(chip(1 - x, cy, cz)))
-    for off in range(1, peers):
-        come = slot_of((s + off) % peers)
-        ref = bound.at[come]
-        remote(ref, ref, own_sem, b_recv.at[come], s, t).wait_recv()
-        store_bound(come)
-
-    for g in range(groups):
-        ref = states.at[g * PLANE + s % PLANE]
-        copy = remote(ref, bound.at[slot], b_send.at[g, 0], b_recv.at[slot], s, t)
-        pl.when(z != g)(copy.wait_send)
-    for copy in sent:
-        copy.wait_send()
-
-    for q in range(PLANE):
-        row = prompt * PLANE + q
-        ref = block_of(row)
-        remote(ref, ref, relay_send.at[q], blk_recv.at[row], s, t).wait_send()
-
-        @pl.when(home)
-        def _():
-            remote(wcross.at[q], ref, cross_send.at[q], blk_recv.at[row], s, t).wait_send()
+    pltpu.make_async_copy(bound.at[far], bound.at[far], b_recv).wait()
+    stored = pltpu.make_async_copy(bound, bound_out, bound_sem)
+    stored.start()
+
+    def sent_all(ref, sem):
+        pltpu.make_async_copy(ref, ref, sem).wait()
+
+    sent_all(xall.at[pl.ds(0, sent["tok"] // PIECES)], tok_send)
+    sent_all(wcross.at[pl.ds(0, PLANE - 1)], w_send)
+    sent_all(wcross, relay_send)
+
+    @pl.when(home)
+    def _():
+        sent_all(wcross, cross_send)
 
     @pl.when(jnp.logical_not(home))
     def _():
-        for cross in (1, 0):
-            for kv in range(2):
-                weight_copies(0, 0, cross, kv)[3].wait_send()
-
-    def give_done(c, carry):
-        exchange(c).wait_send()
-        return carry
-
-    lax.fori_loop(0, peers, give_done, 0)
-    for c in range(peers):
-        pltpu.make_async_copy(final.at[c], final_out.at[c], final_sem.at[c]).wait()
-        pltpu.make_async_copy(bound.at[c], bound_out.at[c], bound_sem.at[c]).wait()
+        sent_all(wcross.at[0], w_away)
+
+    sent_all(gz.at[pl.ds(0, DEEP - 1)], gz_send)
+    sent_all(relayed, g_send)
+    sent_all(give, give_send)
+    sent_all(final.at[pl.ds(0, sent["final"])], f_send)
+    sent_all(states.at[far], b_send)
+    sent_all(rall.at[far], r_send)
+    sent_all(final, final_sem)
+    stored.wait()
 
 
 def prefill(tok, wk, wv, gate_b, gate_a, add, offset, speed, first, strength, gain, readout, peers):
@@ -970,34 +924,31 @@
             pltpu.VMEM((8, readout.shape[1]), f32),
             dma((5,)),
             dma(()),
-            dma((DEEP, PIECES)),
+            dma(()),
             dma((peers, PIECES)),
-            dma((DEEP, PIECES)),
-            dma((DEEP, PIECES)),
-            dma((DEEP,)),
-            dma((DEEP,)),
-            dma((4, 4)),
-            dma((2 * PLANE, 4)),
-            dma((PLANE, 4)),
+            dma(()),
+            dma(()),
             dma((PLANE,)),
             dma((PLANE,)),
+            dma(()),
+            dma(()),
             dma((2 * PLANE,)),
+            dma(()),
             dma((DEEP,)),
-            dma((DEEP,)),
-            dma((DEEP, PLANE)),
+            dma(()),
+            dma(()),
+            dma(()),
+            dma(()),
+            dma(()),
             dma((peers,)),
-            dma((peers,)),
-            dma((peers,)),
-            dma((peers,)),
-            dma((peers,)),
-            dma((DEEP, PLANE)),
-            dma((peers,)),
-            dma((peers,)),
-            dma((peers,)),
-            dma(()),
-            dma(()),
-            dma((peers,)),
-            dma((peers,)),
+            dma(()),
+            dma(()),
+            dma(()),
+            dma(()),
+            dma(()),
+            dma(()),
+            dma(()),
+            dma(()),
         ],
         compiler_params=pltpu.CompilerParams(has_side_effects=True, collective_id=0),
         name="prefill",

time: 101 us -> 96.5 us (0.955)
  Pallas kernels: 99.2 us -> 95.6 us
    pallas_call x1, Pallas kernels: 97.2 us -> 93.6 us  [prefill(): pl.pallas_call(lambda *refs: prefill_kernel(peers, *refs), out_shape=(jax...]
where the time goes in v4:
time: 96.5 us; the launch traced here: 96.3 us
  Pallas kernels  95.6 us (99%)
    pallas_call x1, Pallas kernels, prefill(): pl.pallas_call(lambda *refs: prefill_kernel(peers, *refs), out_shape=(jax...  93.6 us
    pallas_call x1, Pallas kernels, hand_over(): pl.pallas_call(kernel, out_shape=tuple((jax.ShapeDtypeStruct(a.shape, a.d...  2.06 us

profile of v4, /device:TPU:0, one launch (start us, length us, event | category | flops | bytes accessed | tf_op | source)
XLA Modules:
  0.0 96.3 jit_solution(7218373822946396213)
XLA Ops:
  0.6 93.6 %prefill.1 = (bf16[16,128,128]{2,1,0:T(8,128)(2,1)}, bf16[16,128,128]{2,1,0:T(8,128)(2,1)}, bf16[2,256]{1,0:T(2,128)(2,1)}) custom-call(bf16[2,64,4096]{2,1,0:T(8,128)(2,1)} %refs_0_.1, bf16[256,1024]{1,0:T(8,128)(2,1)} %refs_1_.1, bf16[256,1024]{1,0:T(8,128)(2,1)} %refs_2_.1, bf16[16,4096]{1,0:T(8,128)(2,1)} %bitcast.8, bf16[16,4096]{1,0:T(8,128)(2,1)} %bitcast.9, ...), custom_call_target="tpu_custom_call" | custom-call | tf_op jit(solution)/shard_map/prefill/pallas_call | solution.py:894
  94.2 2.1 %hand_over.1 = (bf16[16,128,128]{2,1,0:T(8,128)(2,1)}, bf16[16,128,128]{2,1,0:T(8,128)(2,1)}, bf16[2,256]{1,0:T(2,128)(2,1)}) custom-call(bf16[16,128,128]{2,1,0:T(8,128)(2,1)} %get-tuple-element.9.refs_0_, bf16[16,128,128]{2,1,0:T(8,128)(2,1)} %get-tuple-element.10.refs_1_, bf16[2,256]{1,0:T(2,128)(2,1)} %get-tuple-element.11.refs_2_), custom_call_target="tpu_custom_call" | custom-call | tf_op jit(solution)/shard_map/hand_over/pallas_call | solution.py:980

commit v5 on v4

--- a/solution.py
+++ b/solution.py
@@ -626,16 +626,16 @@
     spread_column(1)
     on_home(3)
     cross_plane(0)
+    along_z(3, tokv)
+    cross_plane(1)
     pass_gates(1)
     on_land(0, 1)
-    along_z(3, tokv)
     spread_column(2)
-    cross_plane(1)
+    cross_plane(2)
     pass_gates(2)
     on_land(2, 3)
     spread_column(3)
     pass_gates(3)
-    cross_plane(2)
     cross_plane(3)
 
     for n in range(PLANE):
@@ -827,6 +827,11 @@
         arrived(come)
         pass_on(come, y_peer)
         pass_on(come, x_peer)
+    for cz in near:
+        come = slot_of(chip(x, 1 - y, cz))
+        arrived(come)
+        pass_on(come, x_peer)
+
     far = pl.ds(0, peers - 1)
     pltpu.make_async_copy(rall.at[far], rall.at[far], r_recv).wait()
     lines = [
@@ -842,11 +847,6 @@
     swap.start()
     swap.wait()
     mixed[...] = (part[...] + partgot[...])[:2].astype(mixed.dtype)
-
-    for cz in near:
-        come = slot_of(chip(x, 1 - y, cz))
-        arrived(come)
-        pass_on(come, x_peer)
 
     for cz in range(DEEP):
         for cy in range(2):

time: 96.5 us -> 96.1 us (level)
  no operation moved by 1% of the time
where the time goes in v5:
time: 96.1 us; the launch traced here: 95.9 us
  Pallas kernels  95.2 us (99%)
    pallas_call x1, Pallas kernels, prefill(): pl.pallas_call(lambda *refs: prefill_kernel(peers, *refs), out_shape=(jax...  93.2 us
    pallas_call x1, Pallas kernels, hand_over(): pl.pallas_call(kernel, out_shape=tuple((jax.ShapeDtypeStruct(a.shape, a.d...  2.06 us

profile of v5, /device:TPU:0, one launch (start us, length us, event | category | flops | bytes accessed | tf_op | source)
XLA Modules:
  0.0 95.9 jit_solution(8678872129274802981)
XLA Ops:
  0.6 93.2 %prefill.1 = (bf16[16,128,128]{2,1,0:T(8,128)(2,1)}, bf16[16,128,128]{2,1,0:T(8,128)(2,1)}, bf16[2,256]{1,0:T(2,128)(2,1)}) custom-call(bf16[2,64,4096]{2,1,0:T(8,128)(2,1)} %refs_0_.1, bf16[256,1024]{1,0:T(8,128)(2,1)} %refs_1_.1, bf16[256,1024]{1,0:T(8,128)(2,1)} %refs_2_.1, bf16[16,4096]{1,0:T(8,128)(2,1)} %bitcast.8, bf16[16,4096]{1,0:T(8,128)(2,1)} %bitcast.9, ...), custom_call_target="tpu_custom_call" | custom-call | tf_op jit(solution)/shard_map/prefill/pallas_call | solution.py:894
  93.8 2.1 %hand_over.1 = (bf16[16,128,128]{2,1,0:T(8,128)(2,1)}, bf16[16,128,128]{2,1,0:T(8,128)(2,1)}, bf16[2,256]{1,0:T(2,128)(2,1)}) custom-call(bf16[16,128,128]{2,1,0:T(8,128)(2,1)} %get-tuple-element.9.refs_0_, bf16[16,128,128]{2,1,0:T(8,128)(2,1)} %get-tuple-element.10.refs_1_, bf16[2,256]{1,0:T(2,128)(2,1)} %get-tuple-element.11.refs_2_), custom_call_target="tpu_custom_call" | custom-call | tf_op jit(solution)/shard_map/hand_over/pallas_call | solution.py:980
